TPU v7x, 32 devices: a whole 2x2x4 slice. The times are simulated.
32 devices in a mesh: fs: 4 (over y, x), tp: 8 (over z, core).
Axes of the slice: x: 2, y: 2, z: 4, core: 2. Of those that a mesh axis runs over, the one named last changes fastest.
Arguments:
- tokens: bfloat16 [1024, 2048], P('fs', 'tp'), may hold values from -60 to 60
- norm_gain: float32 [2048], P('fs'), may hold values from 0.1 to 1.9
- gate_weight: float32 [4, 2048, 4096], P(None, 'fs', 'tp'), may hold values from -0.125 to 0.125
- up_weight: float32 [4, 2048, 4096], P(None, 'fs', 'tp'), may hold values from -0.125 to 0.125
- down_weight: float32 [4, 2048, 4096], P(None, 'fs', 'tp'), may hold values from -0.125 to 0.125
- route: int32 [1024, 2], P('fs'), may hold values from 0 to 3, all different within a row; in each aligned block of 256 rows (0 to 255, 256 to 511, ...) at most 256 rows name the same one
- route_weight: float32 [1024, 2], P('fs'), may hold values from 0.2 to 1
Outputs:
- mixed: bfloat16 [1024, 2048], P('fs', 'tp')
- gate_new: bfloat16 [4, 2048, 4096], P('fs', None, 'tp')
- up_new: bfloat16 [4, 2048, 4096], P('fs', None, 'tp')
- down_new: bfloat16 [4, 2048, 4096], P('fs', None, 'tp')
Inputs may be any that keep to these rules, and one draw needn't show every extreme that they name: `route`: the 2 experts of a row differ. In each aligned block of 256 rows (the tokens of one index of fs) no expert is named by more than 256 rows, a bound that some block reaches.
All inputs are finite; a program needn't handle non-finite values.
Results may differ from a plain program's by a relative error of at most 0.024.
Values may be sent and summed in bfloat16 or wider, within the bound.
A program may use at most 64 MiB of HBM per device.

v0:
```python
import functools

import jax
import jax.numpy as jnp
from jax import lax
from jax.experimental import pallas as pl
from jax.experimental.pallas import tpu as pltpu
from jax.sharding import PartitionSpec as P

epsilon = 1e-05


def slot_table(route, block_rows, expert_count):
    pair_ids = route.reshape(-1, block_rows * route.shape[1])
    onehot = (
        pair_ids[:, :, None] == jnp.arange(expert_count, dtype=jnp.int32)[None, None, :]
    ).astype(jnp.int32)
    before = jnp.cumsum(onehot, axis=1) - onehot
    return jnp.sum(before * onehot, axis=2).reshape(route.shape)


def slotted_body(tokens, norm_gain, gate_weight, up_weight, down_weight, route, route_weight):
    experts = gate_weight.shape[0]
    tok_rows = tokens.shape[0]
    columns = tokens.shape[1]
    fs_count = lax.axis_size("fs")
    capacity = 4 * tok_rows // fs_count
    gain_col = norm_gain[None, :, None]
    gate_cast = (gate_weight * gain_col).astype(jnp.bfloat16)
    up_cast = (up_weight * gain_col).astype(jnp.bfloat16)
    down_cast = down_weight.astype(jnp.bfloat16)
    gate_new, up_new, down_new = (
        lax.all_to_all(gate_cast, "fs", split_axis=0, concat_axis=1, tiled=True),
        lax.all_to_all(up_cast, "fs", split_axis=0, concat_axis=1, tiled=True),
        lax.all_to_all(down_cast, "fs", split_axis=0, concat_axis=1, tiled=True),
    )
    slot_of = slot_table(route, tok_rows, experts)
    target = route * capacity + slot_of
    slot_lanes = jnp.arange(experts * capacity, dtype=jnp.int32)
    slot_hits = target[:, :, None] == slot_lanes[None, None, :]
    token_iota = jnp.arange(tok_rows, dtype=jnp.int32)[:, None, None]
    lane_token = jnp.sum(jnp.where(slot_hits, token_iota + 1, 0), axis=(0, 1)) - 1
    lane_token = jnp.where(lane_token < 0, tok_rows, lane_token)
    combine = jnp.sum(jnp.where(slot_hits, route_weight[:, :, None], 0.0), axis=1)
    tok_float = tokens.astype(jnp.float32)
    square_sum = lax.psum(jnp.sum(tok_float * tok_float, axis=1), "tp")
    full_width = columns * lax.axis_size("tp")
    normed = (tok_float * lax.rsqrt(square_sum / full_width + epsilon)[:, None]).astype(
        jnp.bfloat16
    )
    padded = jnp.concatenate([normed, jnp.zeros((1, columns), jnp.bfloat16)], axis=0)
    outgoing = padded[lane_token].reshape(experts, capacity, columns)
    arrived = lax.all_to_all(outgoing, "fs", split_axis=0, concat_axis=0, tiled=True).reshape(
        -1, columns
    )
    gate_local = gate_new[0]
    up_local = up_new[0]
    piece_rows = lax.all_gather(arrived, "tp", axis=1, tiled=True)
    gate_acc = jnp.dot(piece_rows, gate_local, preferred_element_type=jnp.float32)
    up_acc = jnp.dot(piece_rows, up_local, preferred_element_type=jnp.float32)
    hidden = (jax.nn.silu(gate_acc) * up_acc).astype(jnp.bfloat16)
    down_local = down_new[0]
    summed = lax.psum_scatter(
        lax.dot_general(
            down_local, hidden, (((1,), (1,)), ((), ())), preferred_element_type=jnp.float32
        ).astype(jnp.bfloat16),
        "tp",
        scatter_dimension=0,
        tiled=True,
    ).astype(jnp.float32)
    own_columns = summed.shape[0]
    outgoing_back = summed.astype(jnp.bfloat16).reshape(own_columns, fs_count, capacity)
    returned = lax.all_to_all(outgoing_back, "fs", split_axis=1, concat_axis=1, tiled=True).reshape(
        own_columns, experts * capacity
    )
    mixed = lax.dot_general(
        combine,
        returned.astype(jnp.float32),
        (((1,), (1,)), ((), ())),
        precision=lax.Precision.HIGHEST,
        preferred_element_type=jnp.float32,
    )
    return (mixed.astype(jnp.bfloat16), gate_new, up_new, down_new)


MESH = pl.DeviceIdType.MESH
STAGES = 2
ROW_TILE = 256


def flip(index, distance):
    bit = 1
    while bit <= distance:
        if distance & bit:
            index = index + bit - 2 * bit * ((index // bit) % 2)
        bit *= 2
    return index


def rows_of(index, size):
    return pl.ds(pl.multiple_of(index * size, size), size)


def moe_kernel(
    fs,
    tp,
    tokens,
    gain,
    gate,
    up,
    down,
    route,
    route_weight,
    mixed,
    gate_out,
    up_out,
    down_out,
    loaded,
    staged,
    w_gate,
    w_up,
    w_down,
    tok_raw,
    tok_norm,
    hidden,
    pair_own,
    pair_out,
    pair_in,
    z_out,
    z_in,
    back_out,
    back_in,
    gain_col,
    load_sem,
    tok_local,
    tf_s,
    tf_r,
    tz_s,
    tz_r,
    tw_s,
    tw_r,
    w_s,
    w_r,
    dn_s,
    dn_r,
    pr_s,
    pr_r,
    z_s,
    z_r,
    bk_s,
    bk_r,
    out_sem,
):
    chips = tp // 2
    f = lax.axis_index("fs")
    t = lax.axis_index("tp")
    z, core = t // 2, t % 2
    sibling = flip(t, 1)
    block, width = tokens.shape
    depth, units = gate.shape[1], gate.shape[2]
    sub = width // STAGES
    total_rows = fs * block
    away = [fs - 1] + list(range(1, fs - 1))
    sources, finals = (gate, up, down), (w_gate, w_up, w_down)

    barrier = pltpu.get_barrier_semaphore()
    for d in range(1, fs):
        pl.semaphore_signal(barrier, inc=1, device_id={"fs": flip(f, d)}, device_id_type=MESH)
    for d in range(1, tp):
        pl.semaphore_signal(barrier, inc=1, device_id={"tp": flip(t, d)}, device_id_type=MESH)
    loads = {}
    for p in range(3):
        for d in away + [0]:
            loads[p, d] = pltpu.make_async_copy(
                sources[p].at[flip(f, d)], loaded.at[p, d], load_sem.at[p, d]
            )
            loads[p, d].start()
    own_tok = pltpu.make_async_copy(tokens, tok_raw.at[t, rows_of(f, block)], tok_local)
    own_tok.start()

    gain_col[...] = jnp.broadcast_to(gain[...], (128, depth)).T
    pl.semaphore_wait(barrier, fs + tp - 2)

    sent = []

    def send(src, dst, s_sem, r_sem, **device):
        copy = pltpu.make_async_remote_copy(
            src_ref=src,
            dst_ref=dst,
            send_sem=s_sem,
            recv_sem=r_sem,
            device_id=device,
            device_id_type=MESH,
        )
        copy.start()
        sent.append(copy)
        return copy

    tok_fs = [
        send(tokens, tok_raw.at[t, rows_of(f, block)], tf_s.at[d], tf_r.at[d], fs=flip(f, d))
        for d in away
    ]

    def cast(p, d):
        loads[p, d].wait()
        tile = 64

        @pl.loop(0, depth // tile)
        def _(i):
            rows = rows_of(i, tile)
            value = loaded[p, d, rows, :]
            if p < 2:
                value = value * gain_col[rows, 0:1]
            value = value.astype(jnp.bfloat16)
            if d:
                staged[p, d - 1, rows, :] = value
            else:
                finals[p][pl.ds(pl.multiple_of(f * depth + i * tile, tile), tile), :] = value

    arrive = {}

    def ship(p, d):
        cast(p, d)
        arrive[p, d] = send(
            staged.at[p, d - 1],
            finals[p].at[rows_of(f, depth)],
            w_s.at[p, d],
            w_r.at[p, d],
            fs=flip(f, d),
        )

    for d in away:
        ship(0, d)

    own_tok.wait()
    for copy in tok_fs:
        copy.wait_recv()
    tok_z = {
        d: send(tok_raw.at[t], tok_raw.at[t], tz_s.at[d], tz_r.at[d], tp=flip(t, 2 * d))
        for d in range(1, chips)
    }
    tok_pair = send(tok_raw.at[t], tok_raw.at[t], tz_s.at[0], tz_r.at[0], tp=sibling)

    for d in away:
        ship(1, d)
    for d in away:
        cast(2, d)
    for u in range(STAGES):
        for d in away:
            for c in range(2):
                arrive[2, u, d, c] = send(
                    staged.at[2, d - 1, pl.ds(c * width + u * sub, sub)],
                    w_down.at[
                        pl.ds(pl.multiple_of(f * depth + (c * width + u * sub), sub), sub)
                    ],
                    dn_s.at[u, d, c],
                    dn_r.at[u, d, c],
                    fs=flip(f, d),
                )
    for p in range(3):
        cast(p, 0)

    forwards = []
    for d in range(1, chips):
        tok_z[d].wait_recv()
        there = flip(t, 2 * d)
        forwards.append(
            send(tok_raw.at[there], tok_raw.at[there], tw_s.at[d], tw_r.at[d], tp=sibling)
        )
    tok_pair.wait_recv()
    for copy in forwards:
        copy.wait_recv()

    @pl.loop(0, total_rows // 64)
    def _(i):
        rows = rows_of(i, 64)
        squares = jnp.zeros((64, 1), jnp.float32)
        for k in range(tp):
            value = tok_raw[k, rows, :].astype(jnp.float32)
            squares = squares + jnp.sum(value * value, axis=1, keepdims=True)
        scale = lax.rsqrt(squares / (width * tp) + epsilon)
        for k in range(tp):
            value = tok_raw[k, rows, :].astype(jnp.float32)
            tok_norm[rows, k * width : (k + 1) * width] = (value * scale).astype(jnp.bfloat16)

    for p in range(2):
        for d in away:
            arrive[p, d].wait_recv()
    outs = [
        pltpu.make_async_copy(w_gate, gate_out, out_sem.at[0]),
        pltpu.make_async_copy(w_up, up_out, out_sem.at[1]),
        pltpu.make_async_copy(w_down, down_out, out_sem.at[2]),
    ]
    outs[0].start()
    outs[1].start()

    @pl.loop(0, total_rows // ROW_TILE)
    def _(i):
        rows = rows_of(i, ROW_TILE)
        value = tok_norm[rows, :]
        gate_acc = jnp.dot(value, w_gate[...], preferred_element_type=jnp.float32)
        up_acc = jnp.dot(value, w_up[...], preferred_element_type=jnp.float32)
        hidden[rows, :] = (jax.nn.silu(gate_acc) * up_acc).astype(jnp.bfloat16)

    def product(u, d):
        s = flip(f, d)
        if d:
            for c in range(2):
                arrive[2, u, d, c].wait_recv()

        def weights(c):
            start = pl.multiple_of(s * depth + c * width + u * sub, sub)
            return w_down[pl.ds(start, sub), :]

        @pl.loop(0, total_rows // ROW_TILE)
        def _(i):
            rows = rows_of(i, ROW_TILE)
            value = hidden[rows, :]
            dims = (((1,), (1,)), ((), ()))
            pair_own[u, d, rows, :] = lax.dot_general(
                value, weights(core), dims, preferred_element_type=jnp.float32
            )
            pair_out[u, d, rows, :] = lax.dot_general(
                value, weights(1 - core), dims, preferred_element_type=jnp.float32
            ).astype(jnp.bfloat16)

        return send(
            pair_out.at[u, d], pair_in.at[u, d], pr_s.at[u, d], pr_r.at[u, d], tp=sibling
        )

    z_sends = []

    def pass_on(u, d, copy):
        s = flip(f, d)
        copy.wait_recv()

        def total(rows):
            value = pair_own[u, d, rows, :] + pair_in[u, d, rows, :].astype(jnp.float32)
            return value.astype(jnp.bfloat16)

        @pl.loop(0, total_rows // ROW_TILE)
        def _(i):
            rows = rows_of(i, ROW_TILE)
            z_out[u, d, rows, :] = total(rows)

        across = pltpu.make_async_remote_copy(
            src_ref=z_out.at[u, d],
            dst_ref=z_in.at[u, z],
            send_sem=z_s.at[u, d],
            recv_sem=z_r.at[u, z],
            device_id={"tp": s * 2 + core},
            device_id_type=MESH,
        )

        @pl.when(s != z)
        def _():
            across.start()

        @pl.when(s == z)
        def _():
            @pl.loop(0, total_rows // ROW_TILE)
            def _(i):
                rows = rows_of(i, ROW_TILE)
                z_in[u, z, rows, :] = z_out[u, d, rows, :]

        z_sends.append((s, across))

    returns = []

    def finish(u):
        for d in range(1, chips):
            there = flip(z, d)
            pltpu.make_async_remote_copy(
                src_ref=z_out.at[u, d],
                dst_ref=z_in.at[u, there],
                send_sem=z_s.at[u, d],
                recv_sem=z_r.at[u, there],
                device_id={"tp": there * 2 + core},
                device_id_type=MESH,
            ).wait_recv()
        for d in away + [0]:
            b = flip(f, d)
            rows = rows_of(b, block)
            value = jnp.zeros((block, sub), jnp.float32)
            for k in range(chips):
                value = value + z_in[u, k, rows, :].astype(jnp.float32)
            value = value.astype(jnp.bfloat16)
            if d:
                back_out[u, d] = value
                returns.append(
                    send(
                        back_out.at[u, d],
                        back_in.at[u, f],
                        bk_s.at[u, d],
                        bk_r.at[u, d],
                        fs=b,
                    )
                )
            else:
                back_in[u, f] = value

    items = [(u, 0) for u in range(STAGES)]
    items += [(u, d) for u in range(STAGES) for d in list(range(1, fs - 1)) + [fs - 1]]
    waiting = None
    for item in items:
        copy = product(*item)
        if waiting is not None:
            pass_on(*waiting)
        waiting = item + (copy,)
    outs[2].start()
    pass_on(*waiting)
    for u in range(STAGES):
        finish(u)
    for copy in returns:
        copy.wait_recv()
    for u in range(STAGES):
        value = jnp.zeros((block, sub), jnp.float32)
        for e in range(fs):
            share = jnp.zeros((1, block), jnp.float32)
            for k in range(route.shape[0]):
                share = share + jnp.where(
                    route[k : k + 1, :] == e, route_weight[k : k + 1, :], 0.0
                )
            share = jnp.broadcast_to(share, (sub, block)).T
            value = value + share * back_in[u, e].astype(jnp.float32)
        mixed[:, u * sub : (u + 1) * sub] = value.astype(jnp.bfloat16)

    for copy in sent:
        copy.wait_send()
    for s, across in z_sends:

        @pl.when(s != z)
        def _():
            across.wait_send()

    for copy in outs:
        copy.wait()


def dense_body(tokens, norm_gain, gate_weight, up_weight, down_weight, route, route_weight):
    fs, tp = lax.axis_size("fs"), lax.axis_size("tp")
    block, width = tokens.shape
    experts, depth, units = gate_weight.shape
    rows, full, sub = fs * block, tp * width, width // STAGES
    whole = pl.BlockSpec(memory_space=pltpu.VMEM)
    far = pl.BlockSpec(memory_space=pl.ANY)
    narrow, dma = jnp.bfloat16, pltpu.SemaphoreType.DMA
    weight = jax.ShapeDtypeStruct((full, units), narrow)
    mixed, gate_new, up_new, down_new = pl.pallas_call(
        functools.partial(moe_kernel, fs, tp),
        out_shape=(jax.ShapeDtypeStruct((block, width), narrow), weight, weight, weight),
        in_specs=[whole, whole, far, far, far, whole, whole],
        out_specs=(whole, far, far, far),
        scratch_shapes=[
            pltpu.VMEM((3, experts, depth, units), jnp.float32),
            pltpu.VMEM((3, fs - 1, depth, units), narrow),
            pltpu.VMEM((full, units), narrow),
            pltpu.VMEM((full, units), narrow),
            pltpu.VMEM((full, units), narrow),
            pltpu.VMEM((tp, rows, width), narrow),
            pltpu.VMEM((rows, full), narrow),
            pltpu.VMEM((rows, units), narrow),
            pltpu.VMEM((STAGES, fs, rows, sub), jnp.float32),
            pltpu.VMEM((STAGES, fs, rows, sub), narrow),
            pltpu.VMEM((STAGES, fs, rows, sub), narrow),
            pltpu.VMEM((STAGES, fs, rows, sub), narrow),
            pltpu.VMEM((STAGES, tp // 2, rows, sub), narrow),
            pltpu.VMEM((STAGES, fs, block, sub), narrow),
            pltpu.VMEM((STAGES, fs, block, sub), narrow),
            pltpu.VMEM((depth, 128), jnp.float32),
            dma((3, experts)),
            dma,
            dma((fs,)),
            dma((fs,)),
            dma((tp // 2,)),
            dma((tp // 2,)),
            dma((tp // 2,)),
            dma((tp // 2,)),
            dma((2, fs)),
            dma((2, fs)),
            dma((STAGES, fs, 2)),
            dma((STAGES, fs, 2)),
            dma((STAGES, fs)),
            dma((STAGES, fs)),
            dma((STAGES, fs)),
            dma((STAGES, tp // 2)),
            dma((STAGES, fs)),
            dma((STAGES, fs)),
            dma((3,)),
        ],
        compiler_params=pltpu.CompilerParams(
            collective_id=0, has_side_effects=True, vmem_limit_bytes=64000 * 1024
        ),
    )(tokens, norm_gain[None, :], gate_weight, up_weight, down_weight, route.T, route_weight.T)
    return mixed, gate_new[None], up_new[None], down_new[None]


def body(tokens, norm_gain, gate_weight, up_weight, down_weight, route, route_weight):
    fs, tp = lax.axis_size("fs"), lax.axis_size("tp")
    fits = (
        fs == 4
        and tp == 2 * fs
        and gate_weight.shape[0] == fs
        and tokens.shape[1] % (128 * STAGES) == 0
        and tokens.shape[0] % 64 == 0
        and gate_weight.shape[1] == 2 * tokens.shape[1]
        and tokens.shape[0] * fs * tokens.shape[1] * tp <= 1024 * 2048
    )
    chosen = dense_body if fits else slotted_body
    return chosen(tokens, norm_gain, gate_weight, up_weight, down_weight, route, route_weight)


def solution(mesh):
    in_specs = (
        P("fs", "tp"),
        P("fs"),
        P(None, "fs", "tp"),
        P(None, "fs", "tp"),
        P(None, "fs", "tp"),
        P("fs", None),
        P("fs", None),
    )
    out_specs = (P("fs", "tp"), P("fs", None, "tp"), P("fs", None, "tp"), P("fs", None, "tp"))
    return jax.shard_map(body, mesh=mesh, in_specs=in_specs, out_specs=out_specs, check_vma=False)
```

profile of v0, /device:TPU:0, one launch (start us, length us, event | category | flops | bytes accessed | tf_op | source)
XLA Modules:
  0.0 140.0 jit_solution(9266625817029027459)
XLA Ops:
  0.6 130.9 %shard_map.102 = (bf16[256,256]{1,0:T(8,128)(2,1)}, bf16[2048,512]{1,0:T(8,128)(2,1)}, bf16[2048,512]{1,0:T(8,128)(2,1)}, bf16[2048,512]{1,0:T(8,128)(2,1)}) custom-call(bf16[256,256]{1,0:T(8,128)(2,1)} %tokens.1, f32[1,512]{1,0:T(1,128)} %bitcast.9, f32[4,512,512]{2,1,0:T(8,128)} %gate.1, f32[4,512,512]{2,1,0:T(8,128)} %up.1, f32[4,512,512]{2,1,0:T(8,128)} %down.1, ...), custom_call_target="tpu_custom_call" | custom-call | tf_op jit(solution)/shard_map/pallas_call | solution.py:449
  131.5 1.6 %copy.15 = bf16[256,256]{1,0:T(8,128)(2,1)} copy(bf16[256,256]{1,0:T(8,128)(2,1)} %get-tuple-element.16) | data formatting | bytes 262144
  133.1 0.0 copy-start.1
  133.1 3.2 %copy.16 = bf16[1,2048,512]{2,1,0:T(8,128)(2,1)} copy(bf16[1,2048,512]{2,1,0:T(8,128)(2,1)} %bitcast.8) | data formatting | bytes 4194304
  136.3 0.0 copy-done.1
  136.3 0.0 copy-start
  136.3 1.3 copy.17
  137.6 1.0 copy-done
  138.7 1.3 copy.18
Async XLA Ops:
  133.1 3.2 %copy-start.1 = (bf16[2048,512]{1,0:T(8,128)(2,1)S(1)}, bf16[2048,512]{1,0:T(8,128)(2,1)}, u32[]{:S(2)}) copy-start(bf16[2048,512]{1,0:T(8,128)(2,1)} %get-tuple-element.10) | copy-start | bytes 6291460
  136.3 2.3 %copy-start = (bf16[2048,512]{1,0:T(8,128)(2,1)S(1)}, bf16[2048,512]{1,0:T(8,128)(2,1)}, u32[]{:S(2)}) copy-start(bf16[2048,512]{1,0:T(8,128)(2,1)} %get-tuple-element.11) | copy-start | bytes 6291460
where the time goes:
time: 140 us
  Pallas kernels  131 us (94%)
  local copies, waits for them, and re-layouts  8.43 us (6%)
    pallas_call x1, Pallas kernels, dense_body(): pl.pallas_call(functools.partial(moe_kernel, fs, tp), out_shape=(jax.Shap...  131 us
    unnamed x8, local copies, waits for them, and re-layouts  8.43 us

commit v1 on v0

v1 whole, which is shorter than its diff:
```python
import functools

import jax
import jax.numpy as jnp
from jax import lax
from jax.experimental import pallas as pl
from jax.experimental.pallas import tpu as pltpu
from jax.sharding import PartitionSpec as P

epsilon = 1e-05


def slot_table(route, block_rows, expert_count):
    pair_ids = route.reshape(-1, block_rows * route.shape[1])
    onehot = (
        pair_ids[:, :, None] == jnp.arange(expert_count, dtype=jnp.int32)[None, None, :]
    ).astype(jnp.int32)
    before = jnp.cumsum(onehot, axis=1) - onehot
    return jnp.sum(before * onehot, axis=2).reshape(route.shape)


def slotted_body(tokens, norm_gain, gate_weight, up_weight, down_weight, route, route_weight):
    experts = gate_weight.shape[0]
    tok_rows = tokens.shape[0]
    columns = tokens.shape[1]
    fs_count = lax.axis_size("fs")
    capacity = 4 * tok_rows // fs_count
    gain_col = norm_gain[None, :, None]
    gate_cast = (gate_weight * gain_col).astype(jnp.bfloat16)
    up_cast = (up_weight * gain_col).astype(jnp.bfloat16)
    down_cast = down_weight.astype(jnp.bfloat16)
    gate_new, up_new, down_new = (
        lax.all_to_all(gate_cast, "fs", split_axis=0, concat_axis=1, tiled=True),
        lax.all_to_all(up_cast, "fs", split_axis=0, concat_axis=1, tiled=True),
        lax.all_to_all(down_cast, "fs", split_axis=0, concat_axis=1, tiled=True),
    )
    slot_of = slot_table(route, tok_rows, experts)
    target = route * capacity + slot_of
    slot_lanes = jnp.arange(experts * capacity, dtype=jnp.int32)
    slot_hits = target[:, :, None] == slot_lanes[None, None, :]
    token_iota = jnp.arange(tok_rows, dtype=jnp.int32)[:, None, None]
    lane_token = jnp.sum(jnp.where(slot_hits, token_iota + 1, 0), axis=(0, 1)) - 1
    lane_token = jnp.where(lane_token < 0, tok_rows, lane_token)
    combine = jnp.sum(jnp.where(slot_hits, route_weight[:, :, None], 0.0), axis=1)
    tok_float = tokens.astype(jnp.float32)
    square_sum = lax.psum(jnp.sum(tok_float * tok_float, axis=1), "tp")
    full_width = columns * lax.axis_size("tp")
    normed = (tok_float * lax.rsqrt(square_sum / full_width + epsilon)[:, None]).astype(
        jnp.bfloat16
    )
    padded = jnp.concatenate([normed, jnp.zeros((1, columns), jnp.bfloat16)], axis=0)
    outgoing = padded[lane_token].reshape(experts, capacity, columns)
    arrived = lax.all_to_all(outgoing, "fs", split_axis=0, concat_axis=0, tiled=True).reshape(
        -1, columns
    )
    gate_local = gate_new[0]
    up_local = up_new[0]
    piece_rows = lax.all_gather(arrived, "tp", axis=1, tiled=True)
    gate_acc = jnp.dot(piece_rows, gate_local, preferred_element_type=jnp.float32)
    up_acc = jnp.dot(piece_rows, up_local, preferred_element_type=jnp.float32)
    hidden = (jax.nn.silu(gate_acc) * up_acc).astype(jnp.bfloat16)
    down_local = down_new[0]
    summed = lax.psum_scatter(
        lax.dot_general(
            down_local, hidden, (((1,), (1,)), ((), ())), preferred_element_type=jnp.float32
        ).astype(jnp.bfloat16),
        "tp",
        scatter_dimension=0,
        tiled=True,
    ).astype(jnp.float32)
    own_columns = summed.shape[0]
    outgoing_back = summed.astype(jnp.bfloat16).reshape(own_columns, fs_count, capacity)
    returned = lax.all_to_all(outgoing_back, "fs", split_axis=1, concat_axis=1, tiled=True).reshape(
        own_columns, experts * capacity
    )
    mixed = lax.dot_general(
        combine,
        returned.astype(jnp.float32),
        (((1,), (1,)), ((), ())),
        precision=lax.Precision.HIGHEST,
        preferred_element_type=jnp.float32,
    )
    return (mixed.astype(jnp.bfloat16), gate_new, up_new, down_new)


MESH = pl.DeviceIdType.MESH
STAGES = 2
HALVES = 2
LAG = 2
ROW_TILE = 256
ISSUE = (3, 1, 2)
ARRIVE = (2, 3, 1)


def flip(index, distance):
    bit = 1
    while bit <= distance:
        if distance & bit:
            index = index + bit - 2 * bit * ((index // bit) % 2)
        bit *= 2
    return index


def rows_of(index, size):
    return pl.ds(pl.multiple_of(index * size, size), size)


def moe_kernel(
    fs,
    tp,
    tokens,
    gain,
    gate,
    up,
    down,
    route,
    route_weight,
    mixed,
    gate_out,
    up_out,
    down_out,
    loaded,
    staged,
    w_gate,
    w_up,
    w_down,
    tok,
    gated,
    up_acc,
    hidden,
    pair_own,
    pair_out,
    pair_in,
    chain_in,
    chain_out,
    back_in,
    share,
    mix_out,
    mix_in,
    gain_col,
    load_sem,
    tok_local,
    tf_s,
    tf_r,
    az_s,
    az_r,
    as_s,
    as_r,
    w_s,
    w_r,
    dn_s,
    dn_r,
    pr_s,
    pr_r,
    ch_s,
    ch_r,
    bk_s,
    bk_r,
    mx_s,
    mx_r,
    out_sem,
):
    chips = tp // 2
    last = chips - 1
    f = lax.axis_index("fs")
    t = lax.axis_index("tp")
    z, core = t // 2, t % 2
    sibling = flip(t, 1)
    onward = t + 4 * core - 2
    place = core * z + (1 - core) * (last - z)
    block, width = tokens.shape
    depth, units = gate.shape[1], gate.shape[2]
    sub = width // STAGES
    half = fs * block // HALVES
    sources, finals = (gate, up, down), (w_gate, w_up, w_down)

    barrier = pltpu.get_barrier_semaphore()
    for d in range(1, fs):
        pl.semaphore_signal(barrier, inc=1, device_id={"fs": flip(f, d)}, device_id_type=MESH)
    near = [1] + list(range(2, tp, 2))
    for d in near:
        pl.semaphore_signal(barrier, inc=1, device_id={"tp": flip(t, d)}, device_id_type=MESH)

    def tok_at(k, d):
        return tok.at[k, rows_of(flip(f, d), block)]

    own_tok = pltpu.make_async_copy(tokens, tok_at(t, 0), tok_local)
    own_tok.start()
    loads = {}

    def load(p, d):
        loads[p, d] = pltpu.make_async_copy(
            sources[p].at[flip(f, d)], loaded.at[p, d], load_sem.at[p, d]
        )
        loads[p, d].start()

    for d in ISSUE:
        load(0, d)
    gain_col[...] = jnp.broadcast_to(gain[...], (128, depth)).T
    own_tok.wait()
    pl.semaphore_wait(barrier, fs - 1 + len(near))

    pending = []

    def remote(src, dst, s_sem, r_sem, **device):
        return pltpu.make_async_remote_copy(
            src_ref=src,
            dst_ref=dst,
            send_sem=s_sem,
            recv_sem=r_sem,
            device_id=device,
            device_id_type=MESH,
        )

    def send(*args, **device):
        copy = remote(*args, **device)
        copy.start()
        pending.append((None, copy))
        return copy

    def send_if(condition, *args, **device):
        @pl.when(condition)
        def _():
            remote(*args, **device).start()

        pending.append((condition, (args, device)))

    tok_fs = {
        d: send(tok_at(t, 0), tok_at(t, 0), tf_s.at[d], tf_r.at[d], fs=flip(f, d)) for d in ISSUE
    }

    def spread(d):
        piece = tok_at(t, d)
        send_if(z < last, piece, piece, az_s.at[0, 0, d], az_r.at[z, d], tp=t + 2)
        send_if(z > 0, piece, piece, az_s.at[1, 0, d], az_r.at[z, d], tp=t - 2)
        send(piece, piece, as_s.at[0, 0, d], as_r.at[z, d], tp=sibling)

    def relay(step, d):
        for way in range(2):
            towards = 1 - 2 * way
            here = (z >= step) if way == 0 else (z + step <= last)
            more = (z < last) if way == 0 else (z > 0)
            k = t - 2 * step * towards
            origin = z - step * towards
            piece = tok_at(k, d)

            @pl.when(here)
            def _():
                remote(
                    piece, piece, az_s.at[way, step, d], az_r.at[origin, d], tp=sibling
                ).wait_recv()

            send_if(
                jnp.logical_and(here, more),
                piece,
                piece,
                az_s.at[way, step, d],
                az_r.at[origin, d],
                tp=t + 2 * towards,
            )
            send_if(here, piece, piece, as_s.at[way, step, d], as_r.at[origin, d], tp=sibling)

    def cast(p, d):
        loads[p, d].wait()
        tile = 64

        @pl.loop(0, depth // tile)
        def _(i):
            rows = rows_of(i, tile)
            value = loaded[p, d, rows, :]
            if p < 2:
                value = value * gain_col[rows, 0:1]
            value = value.astype(jnp.bfloat16)
            if d:
                staged[p, d - 1, rows, :] = value
            else:
                finals[p][pl.ds(pl.multiple_of(f * depth + i * tile, tile), tile), :] = value

    arrive = {}

    def ship(p, d):
        cast(p, d)
        arrive[p, d] = send(
            staged.at[p, d - 1],
            finals[p].at[rows_of(f, depth)],
            w_s.at[p, d],
            w_r.at[p, d],
            fs=flip(f, d),
        )

    spread(0)
    for d in ISSUE:
        load(1, d)
    for d in ISSUE:
        ship(0, d)
    for d in ISSUE:
        load(2, d)
    for d in ISSUE:
        tok_fs[d].wait_recv()
        spread(d)
    for d in ISSUE:
        ship(1, d)
    for p in range(3):
        load(p, 0)
    for d in ISSUE:
        cast(2, d)
    for u in range(STAGES):
        for d in ISSUE:
            for c in range(2):
                arrive[2, u, d, c] = send(
                    staged.at[2, d - 1, pl.ds(c * width + u * sub, sub)],
                    w_down.at[
                        pl.ds(pl.multiple_of(f * depth + (c * width + u * sub), sub), sub)
                    ],
                    dn_s.at[u, d, c],
                    dn_r.at[u, d, c],
                    fs=flip(f, d),
                )
    for step in range(1, chips):
        for d in (0,) + ISSUE:
            relay(step, d)
        if step == 1:
            for p in range(3):
                cast(p, 0)
            for e in range(fs):
                part = jnp.zeros((1, block), jnp.float32)
                for k in range(route.shape[0]):
                    part = part + jnp.where(
                        route[k : k + 1, :] == e, route_weight[k : k + 1, :], 0.0
                    )
                share[e] = jnp.broadcast_to(part, (sub, block)).T
    for origin in range(chips):
        for d in (0,) + ISSUE:
            piece = tok_at(2 * origin + 1 - core, d)
            remote(
                piece, piece, as_s.at[0, 0, d], as_r.at[origin, d], tp=sibling
            ).wait_recv()

    for d in ISSUE:
        arrive[0, d].wait_recv()
    outs = [
        pltpu.make_async_copy(w_gate, gate_out, out_sem.at[0]),
        pltpu.make_async_copy(w_up, up_out, out_sem.at[1]),
        pltpu.make_async_copy(w_down, down_out, out_sem.at[2]),
    ]
    outs[0].start()

    @pl.loop(0, fs * block // ROW_TILE)
    def _(i):
        rows = rows_of(i, ROW_TILE)
        parts = [tok[k, rows, :] for k in range(tp)]
        squares = jnp.zeros((ROW_TILE, 1), jnp.float32)
        for part in parts:
            value = part.astype(jnp.float32)
            squares = squares + jnp.sum(value * value, axis=1, keepdims=True)
        scale = lax.rsqrt(squares / (width * tp) + epsilon)
        acc = jnp.dot(
            jnp.concatenate(parts, axis=1), w_gate[...], preferred_element_type=jnp.float32
        )
        gated[rows, :] = jax.nn.silu(acc * scale) * scale

    def up_part(d, rows):
        s = flip(f, d)
        value = jnp.concatenate([tok[2 * s, rows, :], tok[2 * s + 1, rows, :]], axis=1)
        return jnp.dot(value, w_up[rows_of(s, depth), :], preferred_element_type=jnp.float32)

    early = (0,) + ARRIVE[:-1]
    for n, d in enumerate(early):
        if d:
            arrive[1, d].wait_recv()

        @pl.loop(0, fs * block // ROW_TILE)
        def _(i):
            rows = rows_of(i, ROW_TILE)
            part = up_part(d, rows)
            up_acc[rows, :] = up_acc[rows, :] + part if n else part

    arrive[1, ARRIVE[-1]].wait_recv()

    @pl.loop(0, fs * block // ROW_TILE)
    def _(i):
        rows = rows_of(i, ROW_TILE)
        value = up_acc[rows, :] + up_part(ARRIVE[-1], rows)
        hidden[rows, :] = (gated[rows, :] * value).astype(jnp.bfloat16)

    outs[1].start()

    items = [(u, 0) for u in range(STAGES)]
    items += [(u, d) for u in range(STAGES) for d in ARRIVE]
    pieces = [(u, d, h) for u, d in items for h in range(HALVES)]
    count = len(pieces)

    def product(q):
        u, d, h = pieces[q]
        s = flip(f, d)
        if d and h == 0:
            for c in range(2):
                arrive[2, u, d, c].wait_recv()

        def weights(c):
            start = pl.multiple_of(s * depth + c * width + u * sub, sub)
            return w_down[pl.ds(start, sub), :]

        @pl.loop(0, half // ROW_TILE)
        def _(i):
            rows = rows_of(i, ROW_TILE)
            value = hidden[pl.ds(pl.multiple_of(h * half + i * ROW_TILE, ROW_TILE), ROW_TILE), :]
            result = lax.dot_general(
                value,
                jnp.concatenate([weights(core), weights(1 - core)], axis=0),
                (((1,), (1,)), ((), ())),
                preferred_element_type=jnp.float32,
            )
            pair_own[q, rows, :] = result[:, :sub]
            pair_out[q, rows, :] = result[:, sub:].astype(jnp.bfloat16)

        send(pair_out.at[q], pair_in.at[q], pr_s.at[q], pr_r.at[q], tp=sibling)

    per_half = half // block

    def advance(p, j):
        u, d, h = pieces[j]
        s = flip(f, d)
        remote(
            pair_out.at[j], pair_in.at[j], pr_s.at[j], pr_r.at[j], tp=sibling
        ).wait_recv()
        onto = (chain_out.at[j], chain_in.at[j], ch_s.at[j], ch_r.at[j])
        if p:
            remote(*onto, tp=sibling).wait_recv()

        @pl.loop(0, half // ROW_TILE)
        def _(i):
            rows = rows_of(i, ROW_TILE)
            value = pair_own[j, rows, :] + pair_in[j, rows, :].astype(jnp.float32)
            if p:
                value = value + chain_in[j, rows, :].astype(jnp.float32)
            chain_out[j, rows, :] = value.astype(jnp.bfloat16)

        if p < last:
            remote(*onto, tp=onward).start()
            return
        for n in range(per_half):
            b = h * per_half + n
            rows = pl.ds(n * block, block)

            @pl.when(f != b)
            def _():
                remote(
                    chain_out.at[j, rows],
                    back_in.at[u, s, f],
                    bk_s.at[j, n],
                    bk_r.at[u, s, f],
                    fs=b,
                ).start()

            @pl.when(f == b)
            def _():
                back_in[u, s, f] = chain_out[j, rows, :]

    def combine(u):
        for e in range(fs):

            @pl.when(e != f)
            def _():
                for s in range(fs):
                    remote(
                        back_in.at[u, s, e],
                        back_in.at[u, s, e],
                        bk_s.at[0, 0],
                        bk_r.at[u, s, e],
                        fs=flip(f, 1),
                    ).wait_recv()

        for s in range(fs):
            value = jnp.zeros((block, sub), jnp.float32)
            for e in range(fs):
                value = value + share[e] * back_in[u, s, e].astype(jnp.float32)
            value = value.astype(jnp.bfloat16)

            @pl.when(s == z)
            def _():
                mix_in[u] = value

            @pl.when(s != z)
            def _():
                mix_out[u, s] = value
                remote(
                    mix_out.at[u, s], mix_in.at[u], mx_s.at[u, s], mx_r.at[u], tp=2 * s + core
                ).start()

    ready = {}
    for u in range(STAGES):
        done = max(j for j in range(count) if pieces[j][0] == u) + 1 + LAG * last
        ready[min(done + 1, count + LAG * last)] = ready.get(
            min(done + 1, count + LAG * last), []
        ) + [u]
    for q in range(count + 1 + LAG * last):
        if q < count:
            product(q)
        if q == count:
            outs[2].start()
        for p in range(chips):
            j = q - 1 - LAG * p
            if 0 <= j < count:

                @pl.when(place == p)
                def _():
                    advance(p, j)

        for u in ready.get(q, []):

            @pl.when(place == last)
            def _():
                combine(u)

    @pl.when(place < last)
    def _():
        for u in range(STAGES):
            remote(
                mix_out.at[u, 0], mix_in.at[u], mx_s.at[u, 0], mx_r.at[u], tp=sibling
            ).wait_recv()

    for u in range(STAGES):
        mixed[:, u * sub : (u + 1) * sub] = mix_in[u]

    for condition, copy in pending:
        if condition is None:
            copy.wait_send()
        else:

            @pl.when(condition)
            def _():
                args, device = copy
                remote(*args, **device).wait_send()

    @pl.when(place < last)
    def _():
        for j in range(count):
            remote(
                chain_out.at[j], chain_in.at[j], ch_s.at[j], ch_r.at[j], tp=sibling
            ).wait_send()

    @pl.when(place == last)
    def _():
        for j in range(count):
            u, d, h = pieces[j]
            for n in range(per_half):
                b = h * per_half + n

                @pl.when(f != b)
                def _():
                    remote(
                        chain_out.at[j, pl.ds(n * block, block)],
                        back_in.at[u, 0, f],
                        bk_s.at[j, n],
                        bk_r.at[u, 0, f],
                        fs=b,
                    ).wait_send()

        for u in range(STAGES):
            for s in range(fs):

                @pl.when(s != z)
                def _():
                    remote(
                        mix_out.at[u, s], mix_in.at[u], mx_s.at[u, s], mx_r.at[u], tp=sibling
                    ).wait_send()

    for copy in outs:
        copy.wait()


def dense_body(tokens, norm_gain, gate_weight, up_weight, down_weight, route, route_weight):
    fs, tp = lax.axis_size("fs"), lax.axis_size("tp")
    block, width = tokens.shape
    experts, depth, units = gate_weight.shape
    rows, full, sub, chips = fs * block, tp * width, width // STAGES, tp // 2
    count, half = STAGES * fs * HALVES, rows // HALVES
    whole = pl.BlockSpec(memory_space=pltpu.VMEM)
    far = pl.BlockSpec(memory_space=pl.ANY)
    narrow, wide, dma = jnp.bfloat16, jnp.float32, pltpu.SemaphoreType.DMA
    weight = jax.ShapeDtypeStruct((full, units), narrow)
    mixed, gate_new, up_new, down_new = pl.pallas_call(
        functools.partial(moe_kernel, fs, tp),
        out_shape=(jax.ShapeDtypeStruct((block, width), narrow), weight, weight, weight),
        in_specs=[far, whole, far, far, far, whole, whole],
        out_specs=(whole, far, far, far),
        scratch_shapes=[
            pltpu.VMEM((3, experts, depth, units), wide),
            pltpu.VMEM((3, fs - 1, depth, units), narrow),
            pltpu.VMEM((full, units), narrow),
            pltpu.VMEM((full, units), narrow),
            pltpu.VMEM((full, units), narrow),
            pltpu.VMEM((tp, rows, width), narrow),
            pltpu.VMEM((rows, units), wide),
            pltpu.VMEM((rows, units), wide),
            pltpu.VMEM((rows, units), narrow),
            pltpu.VMEM((count, half, sub), wide),
            pltpu.VMEM((count, half, sub), narrow),
            pltpu.VMEM((count, half, sub), narrow),
            pltpu.VMEM((count, half, sub), narrow),
            pltpu.VMEM((count, half, sub), narrow),
            pltpu.VMEM((STAGES, fs, fs, block, sub), narrow),
            pltpu.VMEM((fs, block, sub), wide),
            pltpu.VMEM((STAGES, fs, block, sub), narrow),
            pltpu.VMEM((STAGES, block, sub), narrow),
            pltpu.VMEM((depth, 128), wide),
            dma((3, experts)),
            dma,
            dma((fs,)),
            dma((fs,)),
            dma((2, chips, fs)),
            dma((chips, fs)),
            dma((2, chips, fs)),
            dma((chips, fs)),
            dma((2, fs)),
            dma((2, fs)),
            dma((STAGES, fs, 2)),
            dma((STAGES, fs, 2)),
            dma((count,)),
            dma((count,)),
            dma((count,)),
            dma((count,)),
            dma((count, fs // HALVES)),
            dma((STAGES, fs, fs)),
            dma((STAGES, fs)),
            dma((STAGES,)),
            dma((3,)),
        ],
        compiler_params=pltpu.CompilerParams(
            collective_id=0, has_side_effects=True, vmem_limit_bytes=64000 * 1024
        ),
    )(tokens, norm_gain[None, :], gate_weight, up_weight, down_weight, route.T, route_weight.T)
    return mixed, gate_new[None], up_new[None], down_new[None]


def body(tokens, norm_gain, gate_weight, up_weight, down_weight, route, route_weight):
    fs, tp = lax.axis_size("fs"), lax.axis_size("tp")
    fits = (
        fs == 4
        and tp == 2 * fs
        and gate_weight.shape[0] == fs
        and tokens.shape[1] % (128 * STAGES) == 0
        and tokens.shape[0] % ROW_TILE == 0
        and gate_weight.shape[1] == 2 * tokens.shape[1]
        and tokens.shape[0] * fs * tokens.shape[1] * tp <= 1024 * 2048
    )
    chosen = dense_body if fits else slotted_body
    return chosen(tokens, norm_gain, gate_weight, up_weight, down_weight, route, route_weight)


def solution(mesh):
    in_specs = (
        P("fs", "tp"),
        P("fs"),
        P(None, "fs", "tp"),
        P(None, "fs", "tp"),
        P(None, "fs", "tp"),
        P("fs", None),
        P("fs", None),
    )
    out_specs = (P("fs", "tp"), P("fs", None, "tp"), P("fs", None, "tp"), P("fs", None, "tp"))
    return jax.shard_map(body, mesh=mesh, in_specs=in_specs, out_specs=out_specs, check_vma=False)
```

time: 140 us -> 123 us (0.88)
  Pallas kernels: 131 us -> 113 us
    pallas_call x1, Pallas kernels: 131 us -> 113 us  [dense_body(): pl.pallas_call(functools.partial(moe_kernel, fs, tp), out_shape=(jax.Shap...]
where the time goes in v1:
time: 123 us; the launch traced here: 122 us
  Pallas kernels  113 us (92%)
  local copies, waits for them, and re-layouts  8.43 us (7%)
    pallas_call x1, Pallas kernels, dense_body(): pl.pallas_call(functools.partial(moe_kernel, fs, tp), out_shape=(jax.Shap...  113 us
    unnamed x8, local copies, waits for them, and re-layouts  8.43 us

profile of v1, /device:TPU:0, one launch (start us, length us, event | category | flops | bytes accessed | tf_op | source)
XLA Modules:
  0.0 122.0 jit_solution(11119698878014544670)
XLA Ops:
  0.6 112.9 %shard_map.102 = (bf16[256,256]{1,0:T(8,128)(2,1)}, bf16[2048,512]{1,0:T(8,128)(2,1)}, bf16[2048,512]{1,0:T(8,128)(2,1)}, bf16[2048,512]{1,0:T(8,128)(2,1)}) custom-call(bf16[256,256]{1,0:T(8,128)(2,1)} %tokens.1, f32[1,512]{1,0:T(1,128)} %bitcast.9, f32[4,512,512]{2,1,0:T(8,128)} %gate.1, f32[4,512,512]{2,1,0:T(8,128)} %up.1, f32[4,512,512]{2,1,0:T(8,128)} %down.1, ...), custom_call_target="tpu_custom_call" | custom-call | tf_op jit(solution)/shard_map/pallas_call | solution.py:583
  113.5 1.6 %copy.15 = bf16[256,256]{1,0:T(8,128)(2,1)} copy(bf16[256,256]{1,0:T(8,128)(2,1)} %get-tuple-element.16) | data formatting | bytes 262144
  115.1 0.0 copy-start.1
  115.1 3.2 %copy.16 = bf16[1,2048,512]{2,1,0:T(8,128)(2,1)} copy(bf16[1,2048,512]{2,1,0:T(8,128)(2,1)} %bitcast.8) | data formatting | bytes 4194304
  118.3 0.0 copy-done.1
  118.3 0.0 copy-start
  118.3 1.3 %copy.17 = bf16[1,2048,512]{2,1,0:T(8,128)(2,1)} copy(bf16[1,2048,512]{2,1,0:T(8,128)(2,1)S(1)} %bitcast.7) | data formatting | bytes 4194304
  119.6 1.0 copy-done
  120.6 1.3 %copy.18 = bf16[1,2048,512]{2,1,0:T(8,128)(2,1)} copy(bf16[1,2048,512]{2,1,0:T(8,128)(2,1)S(1)} %bitcast.6) | data formatting | bytes 4194304
Async XLA Ops:
  115.1 3.2 %copy-start.1 = (bf16[2048,512]{1,0:T(8,128)(2,1)S(1)}, bf16[2048,512]{1,0:T(8,128)(2,1)}, u32[]{:S(2)}) copy-start(bf16[2048,512]{1,0:T(8,128)(2,1)} %get-tuple-element.10) | copy-start | bytes 6291460
  118.3 2.3 %copy-start = (bf16[2048,512]{1,0:T(8,128)(2,1)S(1)}, bf16[2048,512]{1,0:T(8,128)(2,1)}, u32[]{:S(2)}) copy-start(bf16[2048,512]{1,0:T(8,128)(2,1)} %get-tuple-element.11) | copy-start | bytes 6291460

commit v2 on v1

--- a/solution.py
+++ b/solution.py
@@ -86,10 +86,10 @@
 MESH = pl.DeviceIdType.MESH
 STAGES = 2
 HALVES = 2
-LAG = 2
+LAG = 3
 ROW_TILE = 256
 ISSUE = (3, 1, 2)
-ARRIVE = (2, 3, 1)
+ARRIVE = (1, 3, 2)
 
 
 def flip(index, distance):
@@ -116,14 +116,14 @@
     route,
     route_weight,
     mixed,
-    gate_out,
-    up_out,
-    down_out,
-    loaded,
-    staged,
     w_gate,
     w_up,
     w_down,
+    gain_row,
+    routes,
+    weights_of,
+    loaded,
+    staged,
     tok,
     gated,
     up_acc,
@@ -139,7 +139,7 @@
     mix_in,
     gain_col,
     load_sem,
-    tok_local,
+    small_sem,
     tf_s,
     tf_r,
     az_s,
@@ -147,8 +147,8 @@
     as_s,
     as_r,
     w_s,
-    w_r,
-    dn_s,
+    g_r,
+    u_r,
     dn_r,
     pr_s,
     pr_r,
@@ -158,7 +158,6 @@
     bk_r,
     mx_s,
     mx_r,
-    out_sem,
 ):
     chips = tp // 2
     last = chips - 1
@@ -184,8 +183,19 @@
     def tok_at(k, d):
         return tok.at[k, rows_of(flip(f, d), block)]
 
-    own_tok = pltpu.make_async_copy(tokens, tok_at(t, 0), tok_local)
-    own_tok.start()
+    small = [
+        pltpu.make_async_copy(source, target, small_sem.at[n])
+        for n, (source, target) in enumerate(
+            (
+                (tokens, tok_at(t, 0)),
+                (gain, gain_row),
+                (route, routes),
+                (route_weight, weights_of),
+            )
+        )
+    ]
+    for copy in small:
+        copy.start()
     loads = {}
 
     def load(p, d):
@@ -196,11 +206,9 @@
 
     for d in ISSUE:
         load(0, d)
-    gain_col[...] = jnp.broadcast_to(gain[...], (128, depth)).T
-    own_tok.wait()
+    for copy in small:
+        copy.wait()
     pl.semaphore_wait(barrier, fs - 1 + len(near))
-
-    pending = []
 
     def remote(src, dst, s_sem, r_sem, **device):
         return pltpu.make_async_remote_copy(
@@ -215,7 +223,6 @@
     def send(*args, **device):
         copy = remote(*args, **device)
         copy.start()
-        pending.append((None, copy))
         return copy
 
     def send_if(condition, *args, **device):
@@ -223,17 +230,18 @@
         def _():
             remote(*args, **device).start()
 
-        pending.append((condition, (args, device)))
+    def take(ref, sem):
+        pltpu.make_async_copy(ref, ref, sem).wait()
 
     tok_fs = {
-        d: send(tok_at(t, 0), tok_at(t, 0), tf_s.at[d], tf_r.at[d], fs=flip(f, d)) for d in ISSUE
+        d: send(tok_at(t, 0), tok_at(t, 0), tf_s, tf_r.at[d], fs=flip(f, d)) for d in ISSUE
     }
 
     def spread(d):
         piece = tok_at(t, d)
-        send_if(z < last, piece, piece, az_s.at[0, 0, d], az_r.at[z, d], tp=t + 2)
-        send_if(z > 0, piece, piece, az_s.at[1, 0, d], az_r.at[z, d], tp=t - 2)
-        send(piece, piece, as_s.at[0, 0, d], as_r.at[z, d], tp=sibling)
+        send_if(z < last, piece, piece, az_s.at[0], az_r.at[z, d], tp=t + 2)
+        send_if(z > 0, piece, piece, az_s.at[1], az_r.at[z, d], tp=t - 2)
+        send(piece, piece, as_s, as_r, tp=sibling)
 
     def relay(step, d):
         for way in range(2):
@@ -246,19 +254,17 @@
 
             @pl.when(here)
             def _():
-                remote(
-                    piece, piece, az_s.at[way, step, d], az_r.at[origin, d], tp=sibling
-                ).wait_recv()
+                take(piece, az_r.at[origin, d])
 
             send_if(
                 jnp.logical_and(here, more),
                 piece,
                 piece,
-                az_s.at[way, step, d],
+                az_s.at[way],
                 az_r.at[origin, d],
                 tp=t + 2 * towards,
             )
-            send_if(here, piece, piece, as_s.at[way, step, d], as_r.at[origin, d], tp=sibling)
+            send_if(here, piece, piece, as_s, as_r, tp=sibling)
 
     def cast(p, d):
         loads[p, d].wait()
@@ -283,12 +289,13 @@
         arrive[p, d] = send(
             staged.at[p, d - 1],
             finals[p].at[rows_of(f, depth)],
-            w_s.at[p, d],
-            w_r.at[p, d],
+            w_s,
+            u_r.at[d] if p else g_r,
             fs=flip(f, d),
         )
 
     spread(0)
+    gain_col[...] = jnp.broadcast_to(gain_row[...], (128, depth)).T
     for d in ISSUE:
         load(1, d)
     for d in ISSUE:
@@ -312,8 +319,8 @@
                     w_down.at[
                         pl.ds(pl.multiple_of(f * depth + (c * width + u * sub), sub), sub)
                     ],
-                    dn_s.at[u, d, c],
-                    dn_r.at[u, d, c],
+                    w_s,
+                    dn_r.at[u, d],
                     fs=flip(f, d),
                 )
     for step in range(1, chips):
@@ -324,26 +331,13 @@
                 cast(p, 0)
             for e in range(fs):
                 part = jnp.zeros((1, block), jnp.float32)
-                for k in range(route.shape[0]):
+                for k in range(routes.shape[0]):
                     part = part + jnp.where(
-                        route[k : k + 1, :] == e, route_weight[k : k + 1, :], 0.0
+                        routes[k : k + 1, :] == e, weights_of[k : k + 1, :], 0.0
                     )
                 share[e] = jnp.broadcast_to(part, (sub, block)).T
-    for origin in range(chips):
-        for d in (0,) + ISSUE:
-            piece = tok_at(2 * origin + 1 - core, d)
-            remote(
-                piece, piece, as_s.at[0, 0, d], as_r.at[origin, d], tp=sibling
-            ).wait_recv()
-
-    for d in ISSUE:
-        arrive[0, d].wait_recv()
-    outs = [
-        pltpu.make_async_copy(w_gate, gate_out, out_sem.at[0]),
-        pltpu.make_async_copy(w_up, up_out, out_sem.at[1]),
-        pltpu.make_async_copy(w_down, down_out, out_sem.at[2]),
-    ]
-    outs[0].start()
+    take(tok.at[pl.ds(0, chips)], as_r)
+    take(w_gate.at[pl.ds(0, (fs - 1) * depth)], g_r)
 
     @pl.loop(0, fs * block // ROW_TILE)
     def _(i):
@@ -377,25 +371,24 @@
 
     arrive[1, ARRIVE[-1]].wait_recv()
 
-    @pl.loop(0, fs * block // ROW_TILE)
-    def _(i):
-        rows = rows_of(i, ROW_TILE)
-        value = up_acc[rows, :] + up_part(ARRIVE[-1], rows)
-        hidden[rows, :] = (gated[rows, :] * value).astype(jnp.bfloat16)
-
-    outs[1].start()
-
-    items = [(u, 0) for u in range(STAGES)]
-    items += [(u, d) for u in range(STAGES) for d in ARRIVE]
-    pieces = [(u, d, h) for u, d in items for h in range(HALVES)]
+    def finish_hidden(h):
+        @pl.loop(0, half // ROW_TILE)
+        def _(i):
+            rows = pl.ds(pl.multiple_of(h * half + i * ROW_TILE, ROW_TILE), ROW_TILE)
+            value = up_acc[rows, :] + up_part(ARRIVE[-1], rows)
+            hidden[rows, :] = (gated[rows, :] * value).astype(jnp.bfloat16)
+
+    pieces = [(u, 0, h) for h in range(HALVES) for u in range(STAGES)]
+    pieces += [(u, d, h) for u in range(STAGES) for d in ARRIVE for h in range(HALVES)]
     count = len(pieces)
 
     def product(q):
         u, d, h = pieces[q]
         s = flip(f, d)
+        if d == 0 and u == 0:
+            finish_hidden(h)
         if d and h == 0:
-            for c in range(2):
-                arrive[2, u, d, c].wait_recv()
+            take(w_down.at[pl.ds(0, 2 * sub)], dn_r.at[u, d])
 
         def weights(c):
             start = pl.multiple_of(s * depth + c * width + u * sub, sub)
@@ -414,19 +407,16 @@
             pair_own[q, rows, :] = result[:, :sub]
             pair_out[q, rows, :] = result[:, sub:].astype(jnp.bfloat16)
 
-        send(pair_out.at[q], pair_in.at[q], pr_s.at[q], pr_r.at[q], tp=sibling)
+        send(pair_out.at[q], pair_in.at[q], pr_s, pr_r.at[q], tp=sibling)
 
     per_half = half // block
 
     def advance(p, j):
         u, d, h = pieces[j]
         s = flip(f, d)
-        remote(
-            pair_out.at[j], pair_in.at[j], pr_s.at[j], pr_r.at[j], tp=sibling
-        ).wait_recv()
-        onto = (chain_out.at[j], chain_in.at[j], ch_s.at[j], ch_r.at[j])
+        take(pair_in.at[j], pr_r.at[j])
         if p:
-            remote(*onto, tp=sibling).wait_recv()
+            take(chain_in.at[j], ch_r.at[j])
 
         @pl.loop(0, half // ROW_TILE)
         def _(i):
@@ -437,7 +427,7 @@
             chain_out[j, rows, :] = value.astype(jnp.bfloat16)
 
         if p < last:
-            remote(*onto, tp=onward).start()
+            send(chain_out.at[j], chain_in.at[j], ch_s, ch_r.at[j], tp=onward)
             return
         for n in range(per_half):
             b = h * per_half + n
@@ -445,32 +435,14 @@
 
             @pl.when(f != b)
             def _():
-                remote(
-                    chain_out.at[j, rows],
-                    back_in.at[u, s, f],
-                    bk_s.at[j, n],
-                    bk_r.at[u, s, f],
-                    fs=b,
-                ).start()
+                send(chain_out.at[j, rows], back_in.at[u, s, f], bk_s, bk_r.at[u], fs=b)
 
             @pl.when(f == b)
             def _():
                 back_in[u, s, f] = chain_out[j, rows, :]
 
     def combine(u):
-        for e in range(fs):
-
-            @pl.when(e != f)
-            def _():
-                for s in range(fs):
-                    remote(
-                        back_in.at[u, s, e],
-                        back_in.at[u, s, e],
-                        bk_s.at[0, 0],
-                        bk_r.at[u, s, e],
-                        fs=flip(f, 1),
-                    ).wait_recv()
-
+        take(back_in.at[u, :, pl.ds(0, fs - 1)], bk_r.at[u])
         for s in range(fs):
             value = jnp.zeros((block, sub), jnp.float32)
             for e in range(fs):
@@ -484,9 +456,7 @@
             @pl.when(s != z)
             def _():
                 mix_out[u, s] = value
-                remote(
-                    mix_out.at[u, s], mix_in.at[u], mx_s.at[u, s], mx_r.at[u], tp=2 * s + core
-                ).start()
+                send(mix_out.at[u, s], mix_in.at[u], mx_s, mx_r.at[u], tp=2 * s + core)
 
     ready = {}
     for u in range(STAGES):
@@ -497,8 +467,6 @@
     for q in range(count + 1 + LAG * last):
         if q < count:
             product(q)
-        if q == count:
-            outs[2].start()
         for p in range(chips):
             j = q - 1 - LAG * p
             if 0 <= j < count:
@@ -516,58 +484,61 @@
     @pl.when(place < last)
     def _():
         for u in range(STAGES):
-            remote(
-                mix_out.at[u, 0], mix_in.at[u], mx_s.at[u, 0], mx_r.at[u], tp=sibling
-            ).wait_recv()
+            take(mix_in.at[u], mx_r.at[u])
 
     for u in range(STAGES):
         mixed[:, u * sub : (u + 1) * sub] = mix_in[u]
 
-    for condition, copy in pending:
-        if condition is None:
-            copy.wait_send()
-        else:
-
-            @pl.when(condition)
-            def _():
-                args, device = copy
-                remote(*args, **device).wait_send()
+    take(tok.at[0, pl.ds(0, (fs - 1) * block)], tf_s)
+    for n in range(chips):
+
+        @pl.when(z == n)
+        def _():
+            if n < last:
+                take(tok.at[pl.ds(0, 1 + n)], az_s.at[0])
+            if n:
+                take(tok.at[pl.ds(0, chips - n)], az_s.at[1])
+
+    take(tok.at[pl.ds(0, chips)], as_s)
+    take(staged, w_s)
+    take(pair_out, pr_s)
 
     @pl.when(place < last)
     def _():
-        for j in range(count):
-            remote(
-                chain_out.at[j], chain_in.at[j], ch_s.at[j], ch_r.at[j], tp=sibling
-            ).wait_send()
+        take(chain_out, ch_s)
 
     @pl.when(place == last)
     def _():
-        for j in range(count):
-            u, d, h = pieces[j]
-            for n in range(per_half):
-                b = h * per_half + n
-
-                @pl.when(f != b)
-                def _():
-                    remote(
-                        chain_out.at[j, pl.ds(n * block, block)],
-                        back_in.at[u, 0, f],
-                        bk_s.at[j, n],
-                        bk_r.at[u, 0, f],
-                        fs=b,
-                    ).wait_send()
-
-        for u in range(STAGES):
-            for s in range(fs):
-
-                @pl.when(s != z)
-                def _():
-                    remote(
-                        mix_out.at[u, s], mix_in.at[u], mx_s.at[u, s], mx_r.at[u], tp=sibling
-                    ).wait_send()
-
-    for copy in outs:
+        take(back_in.at[:, :, pl.ds(0, fs - 1)], bk_s)
+        take(mix_out.at[:, pl.ds(0, chips - 1)], mx_s)
+
+
+def write_kernel(*refs):
+    sem = refs[-1]
+    count = len(refs) // 2
+    copies = [
+        pltpu.make_async_copy(refs[i], refs[count + i].at[0] if i else refs[count], sem.at[i])
+        for i in range(count)
+    ]
+    for copy in copies:
+        copy.start()
+    for copy in copies:
         copy.wait()
+
+
+def write_out(mixed, *weights):
+    whole = pl.BlockSpec(memory_space=pltpu.VMEM)
+    far = pl.BlockSpec(memory_space=pl.ANY)
+    shapes = [jax.ShapeDtypeStruct(mixed.shape, mixed.dtype)]
+    shapes += [jax.ShapeDtypeStruct((1,) + w.shape, w.dtype) for w in weights]
+    return pl.pallas_call(
+        write_kernel,
+        out_shape=tuple(shapes),
+        in_specs=[whole] * len(shapes),
+        out_specs=tuple([far] * len(shapes)),
+        scratch_shapes=[pltpu.SemaphoreType.DMA((len(shapes),))],
+        compiler_params=pltpu.CompilerParams(vmem_limit_bytes=1024 * 1024),
+    )(mixed, *weights)
 
 
 def dense_body(tokens, norm_gain, gate_weight, up_weight, down_weight, route, route_weight):
@@ -579,18 +550,18 @@
     whole = pl.BlockSpec(memory_space=pltpu.VMEM)
     far = pl.BlockSpec(memory_space=pl.ANY)
     narrow, wide, dma = jnp.bfloat16, jnp.float32, pltpu.SemaphoreType.DMA
-    weight = jax.ShapeDtypeStruct((full, units), narrow)
+    weight = pltpu.VMEM((full, units), narrow)
     mixed, gate_new, up_new, down_new = pl.pallas_call(
         functools.partial(moe_kernel, fs, tp),
-        out_shape=(jax.ShapeDtypeStruct((block, width), narrow), weight, weight, weight),
-        in_specs=[far, whole, far, far, far, whole, whole],
-        out_specs=(whole, far, far, far),
+        out_shape=(pltpu.VMEM((block, width), narrow), weight, weight, weight),
+        in_specs=[far] * 7,
+        out_specs=(whole, whole, whole, whole),
         scratch_shapes=[
+            pltpu.VMEM((1, depth), wide),
+            pltpu.VMEM((route.shape[1], block), jnp.int32),
+            pltpu.VMEM((route.shape[1], block), wide),
             pltpu.VMEM((3, experts, depth, units), wide),
             pltpu.VMEM((3, fs - 1, depth, units), narrow),
-            pltpu.VMEM((full, units), narrow),
-            pltpu.VMEM((full, units), narrow),
-            pltpu.VMEM((full, units), narrow),
             pltpu.VMEM((tp, rows, width), narrow),
             pltpu.VMEM((rows, units), wide),
             pltpu.VMEM((rows, units), wide),
@@ -606,32 +577,31 @@
             pltpu.VMEM((STAGES, block, sub), narrow),
             pltpu.VMEM((depth, 128), wide),
             dma((3, experts)),
+            dma((4,)),
             dma,
             dma((fs,)),
+            dma((2,)),
+            dma((chips, fs)),
+            dma,
+            dma,
+            dma,
+            dma,
             dma((fs,)),
-            dma((2, chips, fs)),
-            dma((chips, fs)),
-            dma((2, chips, fs)),
-            dma((chips, fs)),
-            dma((2, fs)),
-            dma((2, fs)),
-            dma((STAGES, fs, 2)),
-            dma((STAGES, fs, 2)),
+            dma((STAGES, fs)),
+            dma,
             dma((count,)),
+            dma,
             dma((count,)),
-            dma((count,)),
-            dma((count,)),
-            dma((count, fs // HALVES)),
-            dma((STAGES, fs, fs)),
-            dma((STAGES, fs)),
+            dma,
             dma((STAGES,)),
-            dma((3,)),
+            dma,
+            dma((STAGES,)),
         ],
         compiler_params=pltpu.CompilerParams(
-            collective_id=0, has_side_effects=True, vmem_limit_bytes=64000 * 1024
+            collective_id=0, has_side_effects=True, vmem_limit_bytes=56 * 1024 * 1024
         ),
     )(tokens, norm_gain[None, :], gate_weight, up_weight, down_weight, route.T, route_weight.T)
-    return mixed, gate_new[None], up_new[None], down_new[None]
+    return write_out(mixed, gate_new, up_new, down_new)
 
 
 def body(tokens, norm_gain, gate_weight, up_weight, down_weight, route, route_weight):

time: 123 us -> 113 us (0.919)
  local copies, waits for them, and re-layouts: 8.43 us -> 0 us
    unnamed x8 -> x0, local copies, waits for them, and re-layouts: 8.43 us -> none
    pallas_call x1 -> x2, Pallas kernels: 113 us -> 112 us  [the longest x1 109 us: dense_body(): pl.pallas_call(functools.partial(moe_kernel, fs, tp), out_shape=(pltpu.VM...]
where the time goes in v2:
time: 113 us
  Pallas kernels  112 us (99%)
    pallas_call x1, Pallas kernels, dense_body(): pl.pallas_call(functools.partial(moe_kernel, fs, tp), out_shape=(pltpu.VM...  109 us
    pallas_call x1, Pallas kernels, write_out(): pl.pallas_call(write_kernel, out_shape=tuple(shapes), in_specs=[whole] *...  2.78 us

profile of v2, /device:TPU:0, one launch (start us, length us, event | category | flops | bytes accessed | tf_op | source)
XLA Modules:
  0.0 112.6 jit_solution(9290199287048627468)
XLA Ops:
  0.6 109.2 %shard_map.102 = (bf16[256,256]{1,0:T(8,128)(2,1)S(1)}, bf16[2048,512]{1,0:T(8,128)(2,1)S(1)}, bf16[2048,512]{1,0:T(8,128)(2,1)S(1)}, bf16[2048,512]{1,0:T(8,128)(2,1)S(1)}) custom-call(bf16[256,256]{1,0:T(8,128)(2,1)} %tokens.1, f32[1,512]{1,0:T(1,128)} %bitcast.3, f32[4,512,512]{2,1,0:T(8,128)} %gate.1, f32[4,512,512]{2,1,0:T(8,128)} %up.1, ...), custom_call_target="tpu_custom_call" | custom-call | tf_op jit(solution)/shard_map/pallas_call | solution.py:554
  109.9 2.8 %shard_map.103 = (bf16[256,256]{1,0:T(8,128)(2,1)}, bf16[1,2048,512]{2,1,0:T(8,128)(2,1)}, bf16[1,2048,512]{2,1,0:T(8,128)(2,1)}, bf16[1,2048,512]{2,1,0:T(8,128)(2,1)}) custom-call(bf16[256,256]{1,0:T(8,128)(2,1)S(1)} %get-tuple-element.8.refs_0_, bf16[2048,512]{1,0:T(8,128)(2,1)S(1)} %get-tuple-element.9.refs_1_, ...), custom_call_target="tpu_custom_call" | custom-call | tf_op jit(solution)/shard_map/pallas_call | solution.py:534

commit v3 on v2

--- a/solution.py
+++ b/solution.py
@@ -85,11 +85,10 @@
 
 MESH = pl.DeviceIdType.MESH
 STAGES = 2
-HALVES = 2
-LAG = 3
-ROW_TILE = 256
-ISSUE = (3, 1, 2)
-ARRIVE = (1, 3, 2)
+QUARTERS = 4
+ISSUE = (1, 2, 3)
+EXPECTED = (7.0, 13.0, 16.0, 20.0, 22.0, 24.0, 28.0, 30.0, 32.0)
+RETURN = 4
 
 
 def flip(index, distance):
@@ -99,6 +98,29 @@
             index = index + bit - 2 * bit * ((index // bit) % 2)
         bit *= 2
     return index
+
+
+def plan(works, pieces, chips):
+    hop, pair, cost = 4.7, 2.0, 0.5
+    starts, needs, now = [], [{}, {}], 0.0
+    for w, (j, at, sides) in enumerate(works):
+        now = max(now, at)
+        starts.append(now)
+        now = now + cost
+        for side in sides:
+            needs[side][j] = (w, now)
+    steps = [[[] for _ in range(chips)] for _ in works]
+    before = [0.0] * pieces
+    for p in range(chips):
+        side, leave, floor = 2 * p // chips, 0.0, 0
+        for j in range(pieces):
+            w, done = needs[side][j]
+            there = max(done + pair, before[j] + hop if p else 0.0)
+            floor = max([floor, w] + [i for i, begin in enumerate(starts) if begin <= there])
+            steps[floor][p].append(j)
+            leave = max(leave + 1.0, there)
+            before[j] = leave
+    return steps
 
 
 def rows_of(index, size):
@@ -167,10 +189,12 @@
     sibling = flip(t, 1)
     onward = t + 4 * core - 2
     place = core * z + (1 - core) * (last - z)
-    block, width = tokens.shape
+    strip, width = tokens.shape[1], tokens.shape[2]
     depth, units = gate.shape[1], gate.shape[2]
+    block, rows_all = QUARTERS * strip, fs * QUARTERS * strip
     sub = width // STAGES
-    half = fs * block // HALVES
+    piece_rows = fs * strip
+    first = 1 - z // (chips // 2)
     sources, finals = (gate, up, down), (w_gate, w_up, w_down)
 
     barrier = pltpu.get_barrier_semaphore()
@@ -181,7 +205,7 @@
         pl.semaphore_signal(barrier, inc=1, device_id={"tp": flip(t, d)}, device_id_type=MESH)
 
     def tok_at(k, d):
-        return tok.at[k, rows_of(flip(f, d), block)]
+        return tok.at[k, :, flip(f, d)]
 
     small = [
         pltpu.make_async_copy(source, target, small_sem.at[n])
@@ -311,18 +335,23 @@
         load(p, 0)
     for d in ISSUE:
         cast(2, d)
-    for u in range(STAGES):
+    def send_down(u, d, c, r_sem):
+        send(
+            staged.at[2, d - 1, pl.ds(pl.multiple_of(c * width + u * sub, sub), sub)],
+            w_down.at[pl.ds(pl.multiple_of(f * depth + c * width + u * sub, sub), sub)],
+            w_s,
+            r_sem,
+            fs=flip(f, d),
+        )
+
+    for u in range(STAGES - 1):
         for d in ISSUE:
             for c in range(2):
-                arrive[2, u, d, c] = send(
-                    staged.at[2, d - 1, pl.ds(c * width + u * sub, sub)],
-                    w_down.at[
-                        pl.ds(pl.multiple_of(f * depth + (c * width + u * sub), sub), sub)
-                    ],
-                    w_s,
-                    dn_r.at[u, d],
-                    fs=flip(f, d),
-                )
+                send_down(u, d, c, dn_r.at[u, d])
+    for side in range(2):
+        for d in ISSUE:
+            c = 1 - first if side else first
+            send_down(STAGES - 1, d, c, dn_r.at[STAGES - 1 + side, d])
     for step in range(1, chips):
         for d in (0,) + ISSUE:
             relay(step, d)
@@ -339,11 +368,14 @@
     take(tok.at[pl.ds(0, chips)], as_r)
     take(w_gate.at[pl.ds(0, (fs - 1) * depth)], g_r)
 
-    @pl.loop(0, fs * block // ROW_TILE)
+    def tok_rows(k, i):
+        return tok[k, i].reshape(piece_rows, width)
+
+    @pl.loop(0, QUARTERS)
     def _(i):
-        rows = rows_of(i, ROW_TILE)
-        parts = [tok[k, rows, :] for k in range(tp)]
-        squares = jnp.zeros((ROW_TILE, 1), jnp.float32)
+        rows = rows_of(i, piece_rows)
+        parts = [tok_rows(k, i) for k in range(tp)]
+        squares = jnp.zeros((piece_rows, 1), jnp.float32)
         for part in parts:
             value = part.astype(jnp.float32)
             squares = squares + jnp.sum(value * value, axis=1, keepdims=True)
@@ -353,63 +385,74 @@
         )
         gated[rows, :] = jax.nn.silu(acc * scale) * scale
 
-    def up_part(d, rows):
+    def up_part(d, i):
         s = flip(f, d)
-        value = jnp.concatenate([tok[2 * s, rows, :], tok[2 * s + 1, rows, :]], axis=1)
+        value = jnp.concatenate([tok_rows(2 * s, i), tok_rows(2 * s + 1, i)], axis=1)
         return jnp.dot(value, w_up[rows_of(s, depth), :], preferred_element_type=jnp.float32)
 
-    early = (0,) + ARRIVE[:-1]
+    early = (0,) + ISSUE[:-1]
     for n, d in enumerate(early):
         if d:
             arrive[1, d].wait_recv()
 
-        @pl.loop(0, fs * block // ROW_TILE)
+        @pl.loop(0, QUARTERS)
         def _(i):
-            rows = rows_of(i, ROW_TILE)
-            part = up_part(d, rows)
+            rows = rows_of(i, piece_rows)
+            part = up_part(d, i)
             up_acc[rows, :] = up_acc[rows, :] + part if n else part
 
-    arrive[1, ARRIVE[-1]].wait_recv()
+    arrive[1, ISSUE[-1]].wait_recv()
 
     def finish_hidden(h):
-        @pl.loop(0, half // ROW_TILE)
-        def _(i):
-            rows = pl.ds(pl.multiple_of(h * half + i * ROW_TILE, ROW_TILE), ROW_TILE)
-            value = up_acc[rows, :] + up_part(ARRIVE[-1], rows)
-            hidden[rows, :] = (gated[rows, :] * value).astype(jnp.bfloat16)
-
-    pieces = [(u, 0, h) for h in range(HALVES) for u in range(STAGES)]
-    pieces += [(u, d, h) for u in range(STAGES) for d in ARRIVE for h in range(HALVES)]
+        rows = pl.ds(h * piece_rows, piece_rows)
+        value = up_acc[rows, :] + up_part(ISSUE[-1], h)
+        hidden[rows, :] = (gated[rows, :] * value).astype(jnp.bfloat16)
+
+    end = STAGES - 1
+    pieces = [(u, 0, h) for h in range(QUARTERS) for u in range(STAGES)]
+    pieces += [(u, d, h) for u in range(STAGES) for d in ISSUE for h in range(QUARTERS)]
     count = len(pieces)
 
-    def product(q):
-        u, d, h = pieces[q]
+    def product(j, side):
+        u, d, h = pieces[j]
         s = flip(f, d)
         if d == 0 and u == 0:
             finish_hidden(h)
         if d and h == 0:
-            take(w_down.at[pl.ds(0, 2 * sub)], dn_r.at[u, d])
+            size = 2 * sub if side is None else sub
+            take(w_down.at[pl.ds(0, size)], dn_r.at[u + (side or 0), d])
 
         def weights(c):
             start = pl.multiple_of(s * depth + c * width + u * sub, sub)
             return w_down[pl.ds(start, sub), :]
 
-        @pl.loop(0, half // ROW_TILE)
-        def _(i):
-            rows = rows_of(i, ROW_TILE)
-            value = hidden[pl.ds(pl.multiple_of(h * half + i * ROW_TILE, ROW_TILE), ROW_TILE), :]
-            result = lax.dot_general(
-                value,
-                jnp.concatenate([weights(core), weights(1 - core)], axis=0),
+        def times(weight):
+            return lax.dot_general(
+                hidden[pl.ds(h * piece_rows, piece_rows), :],
+                weight,
                 (((1,), (1,)), ((), ())),
                 preferred_element_type=jnp.float32,
             )
-            pair_own[q, rows, :] = result[:, :sub]
-            pair_out[q, rows, :] = result[:, sub:].astype(jnp.bfloat16)
-
-        send(pair_out.at[q], pair_in.at[q], pr_s, pr_r.at[q], tp=sibling)
-
-    per_half = half // block
+
+        def give(value):
+            pair_out[j] = value.astype(jnp.bfloat16)
+            send(pair_out.at[j], pair_in.at[j], pr_s, pr_r.at[j], tp=sibling)
+
+        if side is None:
+            result = times(jnp.concatenate([weights(core), weights(1 - core)], axis=0))
+            pair_own[j] = result[:, :sub]
+            give(result[:, sub:])
+            return
+        c = 1 - first if side else first
+        result = times(weights(c))
+
+        @pl.when(core == c)
+        def _():
+            pair_own[j] = result
+
+        @pl.when(core != c)
+        def _():
+            give(result)
 
     def advance(p, j):
         u, d, h = pieces[j]
@@ -418,78 +461,84 @@
         if p:
             take(chain_in.at[j], ch_r.at[j])
 
-        @pl.loop(0, half // ROW_TILE)
-        def _(i):
-            rows = rows_of(i, ROW_TILE)
-            value = pair_own[j, rows, :] + pair_in[j, rows, :].astype(jnp.float32)
-            if p:
-                value = value + chain_in[j, rows, :].astype(jnp.float32)
-            chain_out[j, rows, :] = value.astype(jnp.bfloat16)
+        value = pair_own[j] + pair_in[j].astype(jnp.float32)
+        if p:
+            value = value + chain_in[j].astype(jnp.float32)
+        chain_out[j] = value.astype(jnp.bfloat16)
 
         if p < last:
             send(chain_out.at[j], chain_in.at[j], ch_s, ch_r.at[j], tp=onward)
             return
-        for n in range(per_half):
-            b = h * per_half + n
-            rows = pl.ds(n * block, block)
+        for b in range(fs):
+            rows = pl.ds(b * strip, strip)
 
             @pl.when(f != b)
             def _():
-                send(chain_out.at[j, rows], back_in.at[u, s, f], bk_s, bk_r.at[u], fs=b)
+                send(chain_out.at[j, rows], back_in.at[u, h, s, f], bk_s, bk_r.at[u, h], fs=b)
 
             @pl.when(f == b)
             def _():
-                back_in[u, s, f] = chain_out[j, rows, :]
-
-    def combine(u):
-        take(back_in.at[u, :, pl.ds(0, fs - 1)], bk_r.at[u])
+                back_in[u, h, s, f] = chain_out[j, rows, :]
+
+    def combine(u, h):
+        take(back_in.at[u, h, :, pl.ds(0, fs - 1)], bk_r.at[u, h])
         for s in range(fs):
-            value = jnp.zeros((block, sub), jnp.float32)
+            value = jnp.zeros((strip, sub), jnp.float32)
             for e in range(fs):
-                value = value + share[e] * back_in[u, s, e].astype(jnp.float32)
+                value = value + share[e, pl.ds(h * strip, strip), :] * back_in[u, h, s, e].astype(
+                    jnp.float32
+                )
             value = value.astype(jnp.bfloat16)
 
             @pl.when(s == z)
             def _():
-                mix_in[u] = value
+                mix_in[u, h] = value
 
             @pl.when(s != z)
             def _():
-                mix_out[u, s] = value
-                send(mix_out.at[u, s], mix_in.at[u], mx_s, mx_r.at[u], tp=2 * s + core)
-
-    ready = {}
+                mix_out[u, h, s] = value
+                send(mix_out.at[u, h, s], mix_in.at[u, h], mx_s, mx_r.at[u, h], tp=2 * s + core)
+
+    works = [(j, 0.0, (0, 1)) for j in range(STAGES * QUARTERS)]
+    times_of = iter(EXPECTED)
+    index = {piece: j for j, piece in enumerate(pieces)}
     for u in range(STAGES):
-        done = max(j for j in range(count) if pieces[j][0] == u) + 1 + LAG * last
-        ready[min(done + 1, count + LAG * last)] = ready.get(
-            min(done + 1, count + LAG * last), []
-        ) + [u]
-    for q in range(count + 1 + LAG * last):
-        if q < count:
-            product(q)
+        for side in (0, 1) if u == end else (None,):
+            for d in ISSUE:
+                at = next(times_of)
+                sides = (0, 1) if side is None else (side,)
+                works += [(index[u, d, h], at, sides) for h in range(QUARTERS)]
+    steps = plan(works, count, chips)
+    split = {j for j in range(count) if pieces[j][0] == end and pieces[j][1]}
+    waiting = [(u, h) for u in range(STAGES) for h in range(QUARTERS)]
+    for w, (j, _, sides) in enumerate(works):
+        product(j, sides[0] if j in split else None)
         for p in range(chips):
-            j = q - 1 - LAG * p
-            if 0 <= j < count:
-
-                @pl.when(place == p)
-                def _():
-                    advance(p, j)
-
-        for u in ready.get(q, []):
-
-            @pl.when(place == last)
+            if not steps[w][p]:
+                continue
+
+            @pl.when(place == p)
             def _():
-                combine(u)
+                for i in steps[w][p]:
+                    advance(p, i)
+                    if p == last and waiting[0][0] < end and i >= count - len(split) + RETURN:
+                        combine(*waiting.pop(0))
+
+    @pl.when(place == last)
+    def _():
+        for u, h in waiting:
+            combine(u, h)
 
     @pl.when(place < last)
     def _():
         for u in range(STAGES):
-            take(mix_in.at[u], mx_r.at[u])
+            for h in range(QUARTERS):
+                take(mix_in.at[u, h], mx_r.at[u, h])
 
     for u in range(STAGES):
-        mixed[:, u * sub : (u + 1) * sub] = mix_in[u]
-
-    take(tok.at[0, pl.ds(0, (fs - 1) * block)], tf_s)
+        mixed[:, u * sub : (u + 1) * sub] = mix_in[u].reshape(block, sub)
+
+    take(tok.at[0, :, pl.ds(0, fs - 1)], tf_s)
     for n in range(chips):
 
         @pl.when(z == n)
@@ -509,8 +558,8 @@
 
     @pl.when(place == last)
     def _():
-        take(back_in.at[:, :, pl.ds(0, fs - 1)], bk_s)
-        take(mix_out.at[:, pl.ds(0, chips - 1)], mx_s)
+        take(back_in.at[:, :, :, pl.ds(0, fs - 1)], bk_s)
+        take(mix_out.at[:, :, pl.ds(0, chips - 1)], mx_s)
 
 
 def write_kernel(*refs):
@@ -546,7 +595,8 @@
     block, width = tokens.shape
     experts, depth, units = gate_weight.shape
     rows, full, sub, chips = fs * block, tp * width, width // STAGES, tp // 2
-    count, half = STAGES * fs * HALVES, rows // HALVES
+    count, strip = STAGES * fs * QUARTERS, block // QUARTERS
+    piece = fs * strip
     whole = pl.BlockSpec(memory_space=pltpu.VMEM)
     far = pl.BlockSpec(memory_space=pl.ANY)
     narrow, wide, dma = jnp.bfloat16, jnp.float32, pltpu.SemaphoreType.DMA
@@ -562,19 +612,19 @@
             pltpu.VMEM((route.shape[1], block), wide),
             pltpu.VMEM((3, experts, depth, units), wide),
             pltpu.VMEM((3, fs - 1, depth, units), narrow),
-            pltpu.VMEM((tp, rows, width), narrow),
+            pltpu.VMEM((tp, QUARTERS, fs, strip, width), narrow),
             pltpu.VMEM((rows, units), wide),
             pltpu.VMEM((rows, units), wide),
             pltpu.VMEM((rows, units), narrow),
-            pltpu.VMEM((count, half, sub), wide),
-            pltpu.VMEM((count, half, sub), narrow),
-            pltpu.VMEM((count, half, sub), narrow),
-            pltpu.VMEM((count, half, sub), narrow),
-            pltpu.VMEM((count, half, sub), narrow),
-            pltpu.VMEM((STAGES, fs, fs, block, sub), narrow),
+            pltpu.VMEM((count, piece, sub), wide),
+            pltpu.VMEM((count, piece, sub), narrow),
+            pltpu.VMEM((count, piece, sub), narrow),
+            pltpu.VMEM((count, piece, sub), narrow),
+            pltpu.VMEM((count, piece, sub), narrow),
+            pltpu.VMEM((STAGES, QUARTERS, fs, fs, strip, sub), narrow),
             pltpu.VMEM((fs, block, sub), wide),
-            pltpu.VMEM((STAGES, fs, block, sub), narrow),
-            pltpu.VMEM((STAGES, block, sub), narrow),
+            pltpu.VMEM((STAGES, QUARTERS, fs, strip, sub), narrow),
+            pltpu.VMEM((STAGES, QUARTERS, strip, sub), narrow),
             pltpu.VMEM((depth, 128), wide),
             dma((3, experts)),
             dma((4,)),
@@ -587,20 +637,28 @@
             dma,
             dma,
             dma((fs,)),
-            dma((STAGES, fs)),
+            dma((STAGES + 1, fs)),
             dma,
             dma((count,)),
             dma,
             dma((count,)),
             dma,
-            dma((STAGES,)),
-            dma,
-            dma((STAGES,)),
+            dma((STAGES, QUARTERS)),
+            dma,
+            dma((STAGES, QUARTERS)),
         ],
         compiler_params=pltpu.CompilerParams(
             collective_id=0, has_side_effects=True, vmem_limit_bytes=56 * 1024 * 1024
         ),
-    )(tokens, norm_gain[None, :], gate_weight, up_weight, down_weight, route.T, route_weight.T)
+    )(
+        tokens.reshape(QUARTERS, strip, width),
+        norm_gain[None, :],
+        gate_weight,
+        up_weight,
+        down_weight,
+        route.T,
+        route_weight.T,
+    )
     return write_out(mixed, gate_new, up_new, down_new)
 
 
@@ -611,7 +669,7 @@
         and tp == 2 * fs
         and gate_weight.shape[0] == fs
         and tokens.shape[1] % (128 * STAGES) == 0
-        and tokens.shape[0] % ROW_TILE == 0
+        and tokens.shape[0] % (64 * QUARTERS) == 0
         and gate_weight.shape[1] == 2 * tokens.shape[1]
         and tokens.shape[0] * fs * tokens.shape[1] * tp <= 1024 * 2048
     )

time: 113 us -> 105 us (0.929)
  Pallas kernels: 112 us -> 104 us
    pallas_call x1, Pallas kernels: 109 us -> 102 us  [dense_body(): pl.pallas_call(functools.partial(moe_kernel, fs, tp), out_shape=(pltpu.VM...]
where the time goes in v3:
time: 105 us
  Pallas kernels  104 us (99%)
    pallas_call x1, Pallas kernels, dense_body(): pl.pallas_call(functools.partial(moe_kernel, fs, tp), out_shape=(pltpu.VM...  102 us
    pallas_call x1, Pallas kernels, write_out(): pl.pallas_call(write_kernel, out_shape=tuple(shapes), in_specs=[whole] *...  2.78 us

profile of v3, /device:TPU:0, one launch (start us, length us, event | category | flops | bytes accessed | tf_op | source)
XLA Modules:
  0.0 105.0 jit_solution(9686147056065469249)
XLA Ops:
  0.6 101.5 %shard_map.102 = (bf16[256,256]{1,0:T(8,128)(2,1)S(1)}, bf16[2048,512]{1,0:T(8,128)(2,1)S(1)}, bf16[2048,512]{1,0:T(8,128)(2,1)S(1)}, bf16[2048,512]{1,0:T(8,128)(2,1)S(1)}) custom-call(bf16[4,64,256]{2,1,0:T(8,128)(2,1)} %bitcast.4, f32[1,512]{1,0:T(1,128)} %bitcast.5, f32[4,512,512]{2,1,0:T(8,128)} %gate.1, f32[4,512,512]{2,1,0:T(8,128)} %up.1, ...), custom_call_target="tpu_custom_call" | custom-call | tf_op jit(solution)/shard_map/pallas_call | solution.py:604
  102.2 2.8 %shard_map.103 = (bf16[256,256]{1,0:T(8,128)(2,1)}, bf16[1,2048,512]{2,1,0:T(8,128)(2,1)}, bf16[1,2048,512]{2,1,0:T(8,128)(2,1)}, bf16[1,2048,512]{2,1,0:T(8,128)(2,1)}) custom-call(bf16[256,256]{1,0:T(8,128)(2,1)S(1)} %get-tuple-element.8.refs_0_, bf16[2048,512]{1,0:T(8,128)(2,1)S(1)} %get-tuple-element.9.refs_1_, ...), custom_call_target="tpu_custom_call" | custom-call | tf_op jit(solution)/shard_map/pallas_call | solution.py:583

commit v4 on v3

--- a/solution.py
+++ b/solution.py
@@ -101,9 +101,9 @@
 
 
 def plan(works, pieces, chips):
-    hop, pair, cost = 4.7, 2.0, 0.5
+    hop, pair = 4.7, 2.0
     starts, needs, now = [], [{}, {}], 0.0
-    for w, (j, at, sides) in enumerate(works):
+    for w, (j, at, cost, sides) in enumerate(works):
         now = max(now, at)
         starts.append(now)
         now = now + cost
@@ -158,7 +158,6 @@
     back_in,
     share,
     mix_out,
-    mix_in,
     gain_col,
     load_sem,
     small_sem,
@@ -257,9 +256,19 @@
     def take(ref, sem):
         pltpu.make_async_copy(ref, ref, sem).wait()
 
+    beside = ISSUE[:2]
+    across = ISSUE[2]
     tok_fs = {
-        d: send(tok_at(t, 0), tok_at(t, 0), tf_s, tf_r.at[d], fs=flip(f, d)) for d in ISSUE
+        d: send(tok_at(t, 0), tok_at(t, 0), tf_s, tf_r.at[d], fs=flip(f, d)) for d in beside
     }
+
+    def tok_part(n, d):
+        size = QUARTERS // 2
+        return tok.at[t, pl.ds(n * size, size), flip(f, d)]
+
+    def pass_on(n):
+        piece = tok_part(n, beside[n])
+        send(piece, piece, tf_s, tf_r.at[0 if n else across], fs=flip(f, beside[1 - n]))
 
     def spread(d):
         piece = tok_at(t, d)
@@ -322,13 +331,15 @@
     gain_col[...] = jnp.broadcast_to(gain_row[...], (128, depth)).T
     for d in ISSUE:
         load(1, d)
-    for d in ISSUE:
+    for d in beside:
         ship(0, d)
     for d in ISSUE:
         load(2, d)
-    for d in ISSUE:
+    for n, d in enumerate(beside):
         tok_fs[d].wait_recv()
         spread(d)
+        pass_on(n)
+    ship(0, across)
     for d in ISSUE:
         ship(1, d)
     for p in range(3):
@@ -353,7 +364,7 @@
             c = 1 - first if side else first
             send_down(STAGES - 1, d, c, dn_r.at[STAGES - 1 + side, d])
     for step in range(1, chips):
-        for d in (0,) + ISSUE:
+        for d in (0,) + beside:
             relay(step, d)
         if step == 1:
             for p in range(3):
@@ -365,6 +376,12 @@
                         routes[k : k + 1, :] == e, weights_of[k : k + 1, :], 0.0
                     )
                 share[e] = jnp.broadcast_to(part, (sub, block)).T
+        if step == chips - 2:
+            for n in range(2):
+                take(tok_part(n, across), tf_r.at[0 if n else across])
+            spread(across)
+    for step in range(1, chips):
+        relay(step, across)
     take(tok.at[pl.ds(0, chips)], as_r)
     take(w_gate.at[pl.ds(0, (fs - 1) * depth)], g_r)
 
@@ -492,14 +509,14 @@
 
             @pl.when(s == z)
             def _():
-                mix_in[u, h] = value
+                mixed[u, h] = value
 
             @pl.when(s != z)
             def _():
                 mix_out[u, h, s] = value
-                send(mix_out.at[u, h, s], mix_in.at[u, h], mx_s, mx_r.at[u, h], tp=2 * s + core)
-
-    works = [(j, 0.0, (0, 1)) for j in range(STAGES * QUARTERS)]
+                send(mix_out.at[u, h, s], mixed.at[u, h], mx_s, mx_r.at[u, h], tp=2 * s + core)
+
+    works = [(j, 0.0, 0.5 if pieces[j][0] else 1.0, (0, 1)) for j in range(STAGES * QUARTERS)]
     times_of = iter(EXPECTED)
     index = {piece: j for j, piece in enumerate(pieces)}
     for u in range(STAGES):
@@ -507,11 +524,11 @@
             for d in ISSUE:
                 at = next(times_of)
                 sides = (0, 1) if side is None else (side,)
-                works += [(index[u, d, h], at, sides) for h in range(QUARTERS)]
+                works += [(index[u, d, h], at, 0.5, sides) for h in range(QUARTERS)]
     steps = plan(works, count, chips)
     split = {j for j in range(count) if pieces[j][0] == end and pieces[j][1]}
     waiting = [(u, h) for u in range(STAGES) for h in range(QUARTERS)]
-    for w, (j, _, sides) in enumerate(works):
+    for w, (j, _, _, sides) in enumerate(works):
         product(j, sides[0] if j in split else None)
         for p in range(chips):
             if not steps[w][p]:
@@ -533,10 +550,7 @@
     def _():
         for u in range(STAGES):
             for h in range(QUARTERS):
-                take(mix_in.at[u, h], mx_r.at[u, h])
-
-    for u in range(STAGES):
-        mixed[:, u * sub : (u + 1) * sub] = mix_in[u].reshape(block, sub)
+                take(mixed.at[u, h], mx_r.at[u, h])
 
     take(tok.at[0, :, pl.ds(0, fs - 1)], tf_s)
     for n in range(chips):
@@ -562,12 +576,16 @@
         take(mix_out.at[:, :, pl.ds(0, chips - 1)], mx_s)
 
 
-def write_kernel(*refs):
-    sem = refs[-1]
-    count = len(refs) // 2
+def write_kernel(mixed, gate, up, down, mixed_out, gate_out, up_out, down_out, sem):
+    sub = mixed.shape[3]
     copies = [
-        pltpu.make_async_copy(refs[i], refs[count + i].at[0] if i else refs[count], sem.at[i])
-        for i in range(count)
+        pltpu.make_async_copy(mixed.at[u], mixed_out.at[:, :, pl.ds(u * sub, sub)], sem.at[u])
+        for u in range(STAGES)
+    ]
+    pairs = ((gate, gate_out), (up, up_out), (down, down_out))
+    copies += [
+        pltpu.make_async_copy(source, target.at[0], sem.at[STAGES + n])
+        for n, (source, target) in enumerate(pairs)
     ]
     for copy in copies:
         copy.start()
@@ -578,16 +596,18 @@
 def write_out(mixed, *weights):
     whole = pl.BlockSpec(memory_space=pltpu.VMEM)
     far = pl.BlockSpec(memory_space=pl.ANY)
-    shapes = [jax.ShapeDtypeStruct(mixed.shape, mixed.dtype)]
+    stages, quarters, strip, sub = mixed.shape
+    shapes = [jax.ShapeDtypeStruct((quarters, strip, stages * sub), mixed.dtype)]
     shapes += [jax.ShapeDtypeStruct((1,) + w.shape, w.dtype) for w in weights]
-    return pl.pallas_call(
+    mixed, *weights = pl.pallas_call(
         write_kernel,
         out_shape=tuple(shapes),
         in_specs=[whole] * len(shapes),
         out_specs=tuple([far] * len(shapes)),
-        scratch_shapes=[pltpu.SemaphoreType.DMA((len(shapes),))],
+        scratch_shapes=[pltpu.SemaphoreType.DMA((stages + len(weights),))],
         compiler_params=pltpu.CompilerParams(vmem_limit_bytes=1024 * 1024),
     )(mixed, *weights)
+    return (mixed.reshape(quarters * strip, stages * sub), *weights)
 
 
 def dense_body(tokens, norm_gain, gate_weight, up_weight, down_weight, route, route_weight):
@@ -603,7 +623,7 @@
     weight = pltpu.VMEM((full, units), narrow)
     mixed, gate_new, up_new, down_new = pl.pallas_call(
         functools.partial(moe_kernel, fs, tp),
-        out_shape=(pltpu.VMEM((block, width), narrow), weight, weight, weight),
+        out_shape=(pltpu.VMEM((STAGES, QUARTERS, strip, sub), narrow), weight, weight, weight),
         in_specs=[far] * 7,
         out_specs=(whole, whole, whole, whole),
         scratch_shapes=[
@@ -624,7 +644,6 @@
             pltpu.VMEM((STAGES, QUARTERS, fs, fs, strip, sub), narrow),
             pltpu.VMEM((fs, block, sub), wide),
             pltpu.VMEM((STAGES, QUARTERS, fs, strip, sub), narrow),
-            pltpu.VMEM((STAGES, QUARTERS, strip, sub), narrow),
             pltpu.VMEM((depth, 128), wide),
             dma((3, experts)),
             dma((4,)),

time: 105 us -> 104 us (level)
    pallas_call x1, Pallas kernels: 102 us -> 100 us  [dense_body(): pl.pallas_call(functools.partial(moe_kernel, fs, tp), out_shape=(pltpu.VM...]
where the time goes in v4:
time: 104 us
  Pallas kernels  103 us (99%)
    pallas_call x1, Pallas kernels, dense_body(): pl.pallas_call(functools.partial(moe_kernel, fs, tp), out_shape=(pltpu.VM...  100 us
    pallas_call x1, Pallas kernels, write_out(): pl.pallas_call(write_kernel, out_shape=tuple(shapes), in_specs=[whole] *...  2.79 us

profile of v4, /device:TPU:0, one launch (start us, length us, event | category | flops | bytes accessed | tf_op | source)
XLA Modules:
  0.0 103.6 jit_solution(17033460932403428962)
XLA Ops:
  0.6 100.2 %shard_map.102 = (bf16[2,4,64,128]{3,2,1,0:T(8,128)(2,1)S(1)}, bf16[2048,512]{1,0:T(8,128)(2,1)S(1)}, bf16[2048,512]{1,0:T(8,128)(2,1)S(1)}, bf16[2048,512]{1,0:T(8,128)(2,1)S(1)}) custom-call(bf16[4,64,256]{2,1,0:T(8,128)(2,1)} %bitcast.5, f32[1,512]{1,0:T(1,128)} %bitcast.6, f32[4,512,512]{2,1,0:T(8,128)} %gate.1, f32[4,512,512]{2,1,0:T(8,128)} %up.1, ...), custom_call_target="tpu_custom_call" | custom-call | tf_op jit(solution)/shard_map/pallas_call | solution.py:624
  100.8 2.8 %shard_map.103 = (bf16[4,64,256]{2,1,0:T(8,128)(2,1)}, bf16[1,2048,512]{2,1,0:T(8,128)(2,1)}, bf16[1,2048,512]{2,1,0:T(8,128)(2,1)}, bf16[1,2048,512]{2,1,0:T(8,128)(2,1)}) custom-call(bf16[2,4,64,128]{3,2,1,0:T(8,128)(2,1)S(1)} %get-tuple-element.12.mixed, bf16[2048,512]{1,0:T(8,128)(2,1)S(1)} %get-tuple-element.13.gate, ...), custom_call_target="tpu_custom_call" | custom-call | tf_op jit(solution)/shard_map/pallas_call | solution.py:602

commit v5 on v4

--- a/solution.py
+++ b/solution.py
@@ -87,8 +87,7 @@
 STAGES = 2
 QUARTERS = 4
 ISSUE = (1, 2, 3)
-EXPECTED = (7.0, 13.0, 16.0, 20.0, 22.0, 24.0, 28.0, 30.0, 32.0)
-RETURN = 4
+EXPECTED = (7.0, 13.5, 16.0, 19.0, 22.0, 24.0, 27.0, 30.5, 32.0)
 
 
 def flip(index, distance):
@@ -100,7 +99,7 @@
     return index
 
 
-def plan(works, pieces, chips):
+def plan(works, chain, chips):
     hop, pair = 4.7, 2.0
     starts, needs, now = [], [{}, {}], 0.0
     for w, (j, at, cost, sides) in enumerate(works):
@@ -110,10 +109,10 @@
         for side in sides:
             needs[side][j] = (w, now)
     steps = [[[] for _ in range(chips)] for _ in works]
-    before = [0.0] * pieces
+    before = {}
     for p in range(chips):
         side, leave, floor = 2 * p // chips, 0.0, 0
-        for j in range(pieces):
+        for j in chain:
             w, done = needs[side][j]
             there = max(done + pair, before[j] + hop if p else 0.0)
             floor = max([floor, w] + [i for i, begin in enumerate(starts) if begin <= there])
@@ -158,6 +157,9 @@
     back_in,
     share,
     mix_out,
+    side_in,
+    part_out,
+    part_in,
     gain_col,
     load_sem,
     small_sem,
@@ -179,6 +181,10 @@
     bk_r,
     mx_s,
     mx_r,
+    sd_s,
+    sd_r,
+    pt_s,
+    pt_r,
 ):
     chips = tp // 2
     last = chips - 1
@@ -199,6 +205,8 @@
     barrier = pltpu.get_barrier_semaphore()
     for d in range(1, fs):
         pl.semaphore_signal(barrier, inc=1, device_id={"fs": flip(f, d)}, device_id_type=MESH)
+        beyond = {"fs": flip(f, d), "tp": sibling}
+        pl.semaphore_signal(barrier, inc=1, device_id=beyond, device_id_type=MESH)
     near = [1] + list(range(2, tp, 2))
     for d in near:
         pl.semaphore_signal(barrier, inc=1, device_id={"tp": flip(t, d)}, device_id_type=MESH)
@@ -231,7 +239,7 @@
         load(0, d)
     for copy in small:
         copy.wait()
-    pl.semaphore_wait(barrier, fs - 1 + len(near))
+    pl.semaphore_wait(barrier, 2 * (fs - 1) + len(near))
 
     def remote(src, dst, s_sem, r_sem, **device):
         return pltpu.make_async_remote_copy(
@@ -429,6 +437,8 @@
     pieces = [(u, 0, h) for h in range(QUARTERS) for u in range(STAGES)]
     pieces += [(u, d, h) for u in range(STAGES) for d in ISSUE for h in range(QUARTERS)]
     count = len(pieces)
+    late = QUARTERS - 1
+    chain = [j for j, (u, _, h) in enumerate(pieces) if u < end or h < late]
 
     def product(j, side):
         u, d, h = pieces[j]
@@ -488,33 +498,68 @@
             return
         for b in range(fs):
             rows = pl.ds(b * strip, strip)
-
-            @pl.when(f != b)
-            def _():
-                send(chain_out.at[j, rows], back_in.at[u, h, s, f], bk_s, bk_r.at[u, h], fs=b)
-
-            @pl.when(f == b)
-            def _():
-                back_in[u, h, s, f] = chain_out[j, rows, :]
+            send(
+                chain_out.at[j, rows],
+                back_in.at[u, h, s, f],
+                bk_s,
+                bk_r.at[u, h],
+                fs=b,
+                tp=sibling,
+            )
+
+    def mix(shares, h):
+        value = jnp.zeros((strip, sub), jnp.float32)
+        for e in range(fs):
+            rows = pl.ds(h * strip, strip)
+            value = value + share[e, rows, :] * shares[e].astype(jnp.float32)
+        return value.astype(jnp.bfloat16)
 
     def combine(u, h):
-        take(back_in.at[u, h, :, pl.ds(0, fs - 1)], bk_r.at[u, h])
+        take(back_in.at[u, h], bk_r.at[u, h])
         for s in range(fs):
-            value = jnp.zeros((strip, sub), jnp.float32)
-            for e in range(fs):
-                value = value + share[e, pl.ds(h * strip, strip), :] * back_in[u, h, s, e].astype(
-                    jnp.float32
-                )
-            value = value.astype(jnp.bfloat16)
+            mix_out[u, h, s] = mix([back_in[u, h, s, e] for e in range(fs)], h)
+            send(
+                mix_out.at[u, h, s], mixed.at[u, h], mx_s, mx_r.at[u, h], tp=2 * s + 1 - core
+            )
+
+    def offer():
+        for d in (0,) + ISSUE:
+            j = index[end, d, late]
+            s = flip(f, d)
+            take(pair_in.at[j], pr_r.at[j])
+            value = pair_own[j] + pair_in[j].astype(jnp.float32)
+            chain_out[j] = value.astype(jnp.bfloat16)
+            for b in range(fs):
+                rows = pl.ds(b * strip, strip)
+
+                @pl.when(f != b)
+                def _():
+                    send(chain_out.at[j, rows], side_in.at[s, f], sd_s, sd_r, fs=b)
+
+                @pl.when(f == b)
+                def _():
+                    side_in[s, f] = chain_out[j, rows, :]
+
+    def settle():
+        take(side_in.at[:, pl.ds(0, fs - 1)], sd_r)
+        for s in range(fs):
+            value = mix([side_in[s, e] for e in range(fs)], late)
 
             @pl.when(s == z)
             def _():
-                mixed[u, h] = value
+                part_in[s] = value
 
             @pl.when(s != z)
             def _():
-                mix_out[u, h, s] = value
-                send(mix_out.at[u, h, s], mixed.at[u, h], mx_s, mx_r.at[u, h], tp=2 * s + core)
+                part_out[s] = value
+                send(part_out.at[s], part_in.at[z], pt_s, pt_r, tp=2 * s + core)
+
+    def close():
+        take(part_in.at[pl.ds(0, chips - 1)], pt_r)
+        value = jnp.zeros((strip, sub), jnp.float32)
+        for k in range(chips):
+            value = value + part_in[k].astype(jnp.float32)
+        mixed[end, late] = value.astype(jnp.bfloat16)
 
     works = [(j, 0.0, 0.5 if pieces[j][0] else 1.0, (0, 1)) for j in range(STAGES * QUARTERS)]
     times_of = iter(EXPECTED)
@@ -525,32 +570,43 @@
                 at = next(times_of)
                 sides = (0, 1) if side is None else (side,)
                 works += [(index[u, d, h], at, 0.5, sides) for h in range(QUARTERS)]
-    steps = plan(works, count, chips)
+    steps = plan(works, chain, chips)
     split = {j for j in range(count) if pieces[j][0] == end and pieces[j][1]}
-    waiting = [(u, h) for u in range(STAGES) for h in range(QUARTERS)]
     for w, (j, _, _, sides) in enumerate(works):
         product(j, sides[0] if j in split else None)
         for p in range(chips):
-            if not steps[w][p]:
+            todo = steps[w][p]
+            if not todo and w < len(works) - 1:
                 continue
 
             @pl.when(place == p)
             def _():
-                for i in steps[w][p]:
+                for i in todo[:2]:
                     advance(p, i)
-                    if p == last and waiting[0][0] < end and i >= count - len(split) + RETURN:
-                        combine(*waiting.pop(0))
-
-    @pl.when(place == last)
+                if w == len(works) - 1:
+                    offer()
+                for i in todo[2:]:
+                    advance(p, i)
+
+    placed = [(u, h) for u in range(STAGES) for h in range(QUARTERS) if u < end or h < late]
+
+    @pl.when(place == 0)
     def _():
-        for u, h in waiting:
-            combine(u, h)
-
-    @pl.when(place < last)
+        for u, h in placed:
+            if u < end:
+                combine(u, h)
+
+    settle()
+
+    @pl.when(place == 0)
     def _():
-        for u in range(STAGES):
-            for h in range(QUARTERS):
-                take(mixed.at[u, h], mx_r.at[u, h])
+        for u, h in placed:
+            if u == end:
+                combine(u, h)
+
+    close()
+    for u, h in placed:
+        take(mixed.at[u, h], mx_r.at[u, h])
 
     take(tok.at[0, :, pl.ds(0, fs - 1)], tf_s)
     for n in range(chips):
@@ -566,14 +622,21 @@
     take(staged, w_s)
     take(pair_out, pr_s)
 
+    take(side_in.at[:, pl.ds(0, fs - 1)], sd_s)
+    take(part_out.at[pl.ds(0, chips - 1)], pt_s)
+    passed = chain_out.at[pl.ds(0, len(chain))]
+
     @pl.when(place < last)
     def _():
-        take(chain_out, ch_s)
+        take(passed, ch_s)
 
     @pl.when(place == last)
     def _():
-        take(back_in.at[:, :, :, pl.ds(0, fs - 1)], bk_s)
-        take(mix_out.at[:, :, pl.ds(0, chips - 1)], mx_s)
+        take(passed, bk_s)
+
+    @pl.when(place == 0)
+    def _():
+        take(chain_out.at[pl.ds(0, len(placed))], mx_s)
 
 
 def write_kernel(mixed, gate, up, down, mixed_out, gate_out, up_out, down_out, sem):
@@ -644,6 +707,9 @@
             pltpu.VMEM((STAGES, QUARTERS, fs, fs, strip, sub), narrow),
             pltpu.VMEM((fs, block, sub), wide),
             pltpu.VMEM((STAGES, QUARTERS, fs, strip, sub), narrow),
+            pltpu.VMEM((fs, fs, strip, sub), narrow),
+            pltpu.VMEM((fs, strip, sub), narrow),
+            pltpu.VMEM((chips, strip, sub), narrow),
             pltpu.VMEM((depth, 128), wide),
             dma((3, experts)),
             dma((4,)),
@@ -665,6 +731,10 @@
             dma((STAGES, QUARTERS)),
             dma,
             dma((STAGES, QUARTERS)),
+            dma,
+            dma,
+            dma,
+            dma,
         ],
         compiler_params=pltpu.CompilerParams(
             collective_id=0, has_side_effects=True, vmem_limit_bytes=56 * 1024 * 1024

time: 104 us -> 101 us (0.971)
  Pallas kernels: 103 us -> 99.6 us
    pallas_call x1, Pallas kernels: 100 us -> 96.8 us  [dense_body(): pl.pallas_call(functools.partial(moe_kernel, fs, tp), out_shape=(pltpu.VM...]
where the time goes in v5:
time: 101 us; the launch traced here: 100 us
  Pallas kernels  99.6 us (99%)
    pallas_call x1, Pallas kernels, dense_body(): pl.pallas_call(functools.partial(moe_kernel, fs, tp), out_shape=(pltpu.VM...  96.8 us
    pallas_call x1, Pallas kernels, write_out(): pl.pallas_call(write_kernel, out_shape=tuple(shapes), in_specs=[whole] *...  2.79 us

profile of v5, /device:TPU:0, one launch (start us, length us, event | category | flops | bytes accessed | tf_op | source)
XLA Modules:
  0.0 100.3 jit_solution(12811271936759743053)
XLA Ops:
  0.6 96.8 %shard_map.102 = (bf16[2,4,64,128]{3,2,1,0:T(8,128)(2,1)S(1)}, bf16[2048,512]{1,0:T(8,128)(2,1)S(1)}, bf16[2048,512]{1,0:T(8,128)(2,1)S(1)}, bf16[2048,512]{1,0:T(8,128)(2,1)S(1)}) custom-call(bf16[4,64,256]{2,1,0:T(8,128)(2,1)} %bitcast.5, f32[1,512]{1,0:T(1,128)} %bitcast.6, f32[4,512,512]{2,1,0:T(8,128)} %gate.1, f32[4,512,512]{2,1,0:T(8,128)} %up.1, ...), custom_call_target="tpu_custom_call" | custom-call | tf_op jit(solution)/shard_map/pallas_call | solution.py:687
  97.5 2.8 %shard_map.103 = (bf16[4,64,256]{2,1,0:T(8,128)(2,1)}, bf16[1,2048,512]{2,1,0:T(8,128)(2,1)}, bf16[1,2048,512]{2,1,0:T(8,128)(2,1)}, bf16[1,2048,512]{2,1,0:T(8,128)(2,1)}) custom-call(bf16[2,4,64,128]{3,2,1,0:T(8,128)(2,1)S(1)} %get-tuple-element.12.mixed, bf16[2048,512]{1,0:T(8,128)(2,1)S(1)} %get-tuple-element.13.gate, ...), custom_call_target="tpu_custom_call" | custom-call | tf_op jit(solution)/shard_map/pallas_call | solution.py:665

commit v6 on v5

--- a/solution.py
+++ b/solution.py
@@ -99,7 +99,7 @@
     return index
 
 
-def plan(works, chain, chips):
+def plan(works, chain, bundle, chips):
     hop, pair = 4.7, 2.0
     starts, needs, now = [], [{}, {}], 0.0
     for w, (j, at, cost, sides) in enumerate(works):
@@ -113,7 +113,7 @@
     for p in range(chips):
         side, leave, floor = 2 * p // chips, 0.0, 0
         for j in chain:
-            w, done = needs[side][j]
+            w, done = max(needs[side][i] for i in needs[side] if bundle[i] == bundle[j])
             there = max(done + pair, before[j] + hop if p else 0.0)
             floor = max([floor, w] + [i for i, begin in enumerate(starts) if begin <= there])
             steps[floor][p].append(j)
@@ -194,6 +194,9 @@
     sibling = flip(t, 1)
     onward = t + 4 * core - 2
     place = core * z + (1 - core) * (last - z)
+    hub = t - core + 1
+    mixes = jnp.logical_and(core == 1, jnp.logical_or(z == 0, z == last))
+    alone = jnp.logical_and(core == 1, z == last)
     strip, width = tokens.shape[1], tokens.shape[2]
     depth, units = gate.shape[1], gate.shape[2]
     block, rows_all = QUARTERS * strip, fs * QUARTERS * strip
@@ -207,7 +210,7 @@
         pl.semaphore_signal(barrier, inc=1, device_id={"fs": flip(f, d)}, device_id_type=MESH)
         beyond = {"fs": flip(f, d), "tp": sibling}
         pl.semaphore_signal(barrier, inc=1, device_id=beyond, device_id_type=MESH)
-    near = [1] + list(range(2, tp, 2))
+    near = list(range(1, tp))
     for d in near:
         pl.semaphore_signal(barrier, inc=1, device_id={"tp": flip(t, d)}, device_id_type=MESH)
 
@@ -227,13 +230,9 @@
     ]
     for copy in small:
         copy.start()
-    loads = {}
-
     def load(p, d):
-        loads[p, d] = pltpu.make_async_copy(
-            sources[p].at[flip(f, d)], loaded.at[p, d], load_sem.at[p, d]
-        )
-        loads[p, d].start()
+        sem = load_sem.at[p if d else 3]
+        pltpu.make_async_copy(sources[p].at[flip(f, d)], loaded.at[p, d], sem).start()
 
     for d in ISSUE:
         load(0, d)
@@ -308,7 +307,10 @@
             send_if(here, piece, piece, as_s, as_r, tp=sibling)
 
     def cast(p, d):
-        loads[p, d].wait()
+        if d == ISSUE[0]:
+            take(loaded.at[p, pl.ds(1, fs - 1)], load_sem.at[p])
+        elif d == 0 and p == 0:
+            take(loaded.at[:, 0], load_sem.at[3])
         tile = 64
 
         @pl.loop(0, depth // tile)
@@ -331,7 +333,7 @@
             staged.at[p, d - 1],
             finals[p].at[rows_of(f, depth)],
             w_s,
-            u_r.at[d] if p else g_r,
+            u_r.at[d - 1] if p else g_r,
             fs=flip(f, d),
         )
 
@@ -366,11 +368,11 @@
     for u in range(STAGES - 1):
         for d in ISSUE:
             for c in range(2):
-                send_down(u, d, c, dn_r.at[u, d])
-    for side in range(2):
+                send_down(u, d, c, dn_r.at[u, d - 1])
+    for turn in range(2):
         for d in ISSUE:
-            c = 1 - first if side else first
-            send_down(STAGES - 1, d, c, dn_r.at[STAGES - 1 + side, d])
+            c = 1 - first if turn else first
+            send_down(STAGES - 1, d, c, dn_r.at[STAGES - 1 + turn, d - 1])
     for step in range(1, chips):
         for d in (0,) + beside:
             relay(step, d)
@@ -439,15 +441,21 @@
     count = len(pieces)
     late = QUARTERS - 1
     chain = [j for j, (u, _, h) in enumerate(pieces) if u < end or h < late]
-
-    def product(j, side):
+    bundle, lead = {}, {}
+    for j, (u, d, h) in enumerate(pieces):
+        key = late if u == end and h == late else (u, d, h if d == 0 else h // 2 if u < end else 0)
+        bundle[j] = lead.setdefault(key, (len(lead), j))[0]
+    sizes = [list(bundle.values()).count(n) for n in range(len(lead))]
+    leads = {j: n for n, j in lead.values()}
+
+    def product(j, turn):
         u, d, h = pieces[j]
         s = flip(f, d)
         if d == 0 and u == 0:
             finish_hidden(h)
         if d and h == 0:
-            size = 2 * sub if side is None else sub
-            take(w_down.at[pl.ds(0, size)], dn_r.at[u + (side or 0), d])
+            size = 2 * sub if turn is None else sub
+            take(w_down.at[pl.ds(0, size)], dn_r.at[u + (turn or 0), d - 1])
 
         def weights(c):
             start = pl.multiple_of(s * depth + c * width + u * sub, sub)
@@ -463,14 +471,14 @@
 
         def give(value):
             pair_out[j] = value.astype(jnp.bfloat16)
-            send(pair_out.at[j], pair_in.at[j], pr_s, pr_r.at[j], tp=sibling)
-
-        if side is None:
+            send(pair_out.at[j], pair_in.at[j], pr_s, pr_r.at[bundle[j]], tp=sibling)
+
+        if turn is None:
             result = times(jnp.concatenate([weights(core), weights(1 - core)], axis=0))
             pair_own[j] = result[:, :sub]
             give(result[:, sub:])
             return
-        c = 1 - first if side else first
+        c = 1 - first if turn else first
         result = times(weights(c))
 
         @pl.when(core == c)
@@ -484,7 +492,8 @@
     def advance(p, j):
         u, d, h = pieces[j]
         s = flip(f, d)
-        take(pair_in.at[j], pr_r.at[j])
+        if j in leads:
+            take(pair_in.at[pl.ds(j, sizes[leads[j]])], pr_r.at[leads[j]])
         if p:
             take(chain_in.at[j], ch_r.at[j])
 
@@ -498,14 +507,22 @@
             return
         for b in range(fs):
             rows = pl.ds(b * strip, strip)
-            send(
-                chain_out.at[j, rows],
-                back_in.at[u, h, s, f],
-                bk_s,
-                bk_r.at[u, h],
-                fs=b,
-                tp=sibling,
-            )
+            here = jnp.logical_and(f == b, core == 1)
+
+            @pl.when(here)
+            def _():
+                back_in[u, h, s, f] = chain_out[j, rows, :]
+
+            @pl.when(jnp.logical_not(here))
+            def _():
+                send(
+                    chain_out.at[j, rows],
+                    back_in.at[u, h, s, f],
+                    bk_s,
+                    bk_r.at[1 + h if u == end else u],
+                    fs=b,
+                    tp=hub,
+                )
 
     def mix(shares, h):
         value = jnp.zeros((strip, sub), jnp.float32)
@@ -515,18 +532,39 @@
         return value.astype(jnp.bfloat16)
 
     def combine(u, h):
-        take(back_in.at[u, h], bk_r.at[u, h])
+        @pl.when(alone)
+        def _():
+            if u == end:
+                take(back_in.at[u, h, :, pl.ds(0, fs - 1)], bk_r.at[1 + h])
+            elif h == 0:
+                take(back_in.at[u, :, :, pl.ds(0, fs - 1)], bk_r.at[u])
+
+        @pl.when(jnp.logical_not(alone))
+        def _():
+            if u == end:
+                take(back_in.at[u, h], bk_r.at[1 + h])
+            elif h == 0:
+                take(back_in.at[u], bk_r.at[u])
+
         for s in range(fs):
-            mix_out[u, h, s] = mix([back_in[u, h, s, e] for e in range(fs)], h)
-            send(
-                mix_out.at[u, h, s], mixed.at[u, h], mx_s, mx_r.at[u, h], tp=2 * s + 1 - core
-            )
+            value = mix([back_in[u, h, s, e] for e in range(fs)], h)
+            here = jnp.logical_and(s == z, alone)
+
+            @pl.when(here)
+            def _():
+                mixed[u, h] = value
+
+            @pl.when(jnp.logical_not(here))
+            def _():
+                mix_out[u, h, s] = value
+                send(mix_out.at[u, h, s], mixed.at[u, h], mx_s, mx_r, tp=2 * s + z // last)
 
     def offer():
         for d in (0,) + ISSUE:
             j = index[end, d, late]
             s = flip(f, d)
-            take(pair_in.at[j], pr_r.at[j])
+            if d == 0:
+                take(pair_in.at[pl.ds(0, sizes[bundle[j]])], pr_r.at[bundle[j]])
             value = pair_own[j] + pair_in[j].astype(jnp.float32)
             chain_out[j] = value.astype(jnp.bfloat16)
             for b in range(fs):
@@ -565,15 +603,15 @@
     times_of = iter(EXPECTED)
     index = {piece: j for j, piece in enumerate(pieces)}
     for u in range(STAGES):
-        for side in (0, 1) if u == end else (None,):
+        for turn in (0, 1) if u == end else (None,):
             for d in ISSUE:
                 at = next(times_of)
-                sides = (0, 1) if side is None else (side,)
-                works += [(index[u, d, h], at, 0.5, sides) for h in range(QUARTERS)]
-    steps = plan(works, chain, chips)
+                turns = (0, 1) if turn is None else (turn,)
+                works += [(index[u, d, h], at, 0.5, turns) for h in range(QUARTERS)]
+    steps = plan(works, chain, bundle, chips)
     split = {j for j in range(count) if pieces[j][0] == end and pieces[j][1]}
-    for w, (j, _, _, sides) in enumerate(works):
-        product(j, sides[0] if j in split else None)
+    for w, (j, _, _, turns) in enumerate(works):
+        product(j, turns[0] if j in split else None)
         for p in range(chips):
             todo = steps[w][p]
             if not todo and w < len(works) - 1:
@@ -590,23 +628,18 @@
 
     placed = [(u, h) for u in range(STAGES) for h in range(QUARTERS) if u < end or h < late]
 
-    @pl.when(place == 0)
+    settle()
+
+    @pl.when(mixes)
     def _():
         for u, h in placed:
-            if u < end:
-                combine(u, h)
-
-    settle()
-
-    @pl.when(place == 0)
+            combine(u, h)
+
+    close()
+    @pl.when(jnp.logical_not(alone))
     def _():
-        for u, h in placed:
-            if u == end:
-                combine(u, h)
-
-    close()
-    for u, h in placed:
-        take(mixed.at[u, h], mx_r.at[u, h])
+        take(chain_out.at[pl.ds(0, len(placed)), pl.ds(0, strip)], mx_r)
+
 
     take(tok.at[0, :, pl.ds(0, fs - 1)], tf_s)
     for n in range(chips):
@@ -630,13 +663,18 @@
     def _():
         take(passed, ch_s)
 
-    @pl.when(place == last)
+    @pl.when(jnp.logical_and(place == last, core == 0))
     def _():
         take(passed, bk_s)
 
-    @pl.when(place == 0)
+    @pl.when(jnp.logical_and(mixes, z == 0))
     def _():
         take(chain_out.at[pl.ds(0, len(placed))], mx_s)
+
+    @pl.when(alone)
+    def _():
+        take(chain_out.at[pl.ds(0, len(chain)), pl.ds(0, (fs - 1) * strip)], bk_s)
+        take(chain_out.at[pl.ds(0, len(placed)), pl.ds(0, (fs - 1) * strip)], mx_s)
 
 
 def write_kernel(mixed, gate, up, down, mixed_out, gate_out, up_out, down_out, sem):
@@ -711,7 +749,7 @@
             pltpu.VMEM((fs, strip, sub), narrow),
             pltpu.VMEM((chips, strip, sub), narrow),
             pltpu.VMEM((depth, 128), wide),
-            dma((3, experts)),
+            dma((4,)),
             dma((4,)),
             dma,
             dma((fs,)),
@@ -721,16 +759,16 @@
             dma,
             dma,
             dma,
-            dma((fs,)),
-            dma((STAGES + 1, fs)),
+            dma((fs - 1,)),
+            dma((STAGES + 1, fs - 1)),
+            dma,
+            dma((count // 2 + 1,)),
             dma,
             dma((count,)),
             dma,
-            dma((count,)),
-            dma,
-            dma((STAGES, QUARTERS)),
-            dma,
-            dma((STAGES, QUARTERS)),
+            dma((QUARTERS + 1,)),
+            dma,
+            dma,
             dma,
             dma,
             dma,

time: 101 us -> 101 us (level)
  no operation moved by 1% of the time
where the time goes in v6:
time: 101 us; the launch traced here: 100 us
  Pallas kernels  99.7 us (99%)
    pallas_call x1, Pallas kernels, dense_body(): pl.pallas_call(functools.partial(moe_kernel, fs, tp), out_shape=(pltpu.VM...  96.9 us
    pallas_call x1, Pallas kernels, write_out(): pl.pallas_call(write_kernel, out_shape=tuple(shapes), in_specs=[whole] *...  2.79 us

profile of v6, /device:TPU:0, one launch (start us, length us, event | category | flops | bytes accessed | tf_op | source)
XLA Modules:
  0.0 100.3 jit_solution(16656754640092498519)
XLA Ops:
  0.6 96.9 %shard_map.102 = (bf16[2,4,64,128]{3,2,1,0:T(8,128)(2,1)S(1)}, bf16[2048,512]{1,0:T(8,128)(2,1)S(1)}, bf16[2048,512]{1,0:T(8,128)(2,1)S(1)}, bf16[2048,512]{1,0:T(8,128)(2,1)S(1)}) custom-call(bf16[4,64,256]{2,1,0:T(8,128)(2,1)} %bitcast.5, f32[1,512]{1,0:T(1,128)} %bitcast.6, f32[4,512,512]{2,1,0:T(8,128)} %gate.1, f32[4,512,512]{2,1,0:T(8,128)} %up.1, ...), custom_call_target="tpu_custom_call" | custom-call | tf_op jit(solution)/shard_map/pallas_call | solution.py:725
  97.5 2.8 %shard_map.103 = (bf16[4,64,256]{2,1,0:T(8,128)(2,1)}, bf16[1,2048,512]{2,1,0:T(8,128)(2,1)}, bf16[1,2048,512]{2,1,0:T(8,128)(2,1)}, bf16[1,2048,512]{2,1,0:T(8,128)(2,1)}) custom-call(bf16[2,4,64,128]{3,2,1,0:T(8,128)(2,1)S(1)} %get-tuple-element.12.mixed, bf16[2048,512]{1,0:T(8,128)(2,1)S(1)} %get-tuple-element.13.gate, ...), custom_call_target="tpu_custom_call" | custom-call | tf_op jit(solution)/shard_map/pallas_call | solution.py:703

commit v7 on v6

--- a/solution.py
+++ b/solution.py
@@ -87,7 +87,7 @@
 STAGES = 2
 QUARTERS = 4
 ISSUE = (1, 2, 3)
-EXPECTED = (7.0, 13.5, 16.0, 19.0, 22.0, 24.0, 27.0, 30.5, 32.0)
+EXPECTED = (7.0, 12.0, 15.0, 18.0, 20.0, 22.0, 25.0, 28.0, 30.0)
 
 
 def flip(index, distance):
@@ -100,7 +100,7 @@
 
 
 def plan(works, chain, bundle, chips):
-    hop, pair = 4.7, 2.0
+    hop, pair = 4.0, 2.0
     starts, needs, now = [], [{}, {}], 0.0
     for w, (j, at, cost, sides) in enumerate(works):
         now = max(now, at)

time: 101 us -> 100 us (0.990)
  no operation moved by 1% of the time
where the time goes in v7:
time: 100 us
  Pallas kernels  99.3 us (99%)
    pallas_call x1, Pallas kernels, dense_body(): pl.pallas_call(functools.partial(moe_kernel, fs, tp), out_shape=(pltpu.VM...  96.5 us
    pallas_call x1, Pallas kernels, write_out(): pl.pallas_call(write_kernel, out_shape=tuple(shapes), in_specs=[whole] *...  2.79 us

profile of v7, /device:TPU:0, one launch (start us, length us, event | category | flops | bytes accessed | tf_op | source)
XLA Modules:
  0.0 100.0 jit_solution(10727339888817999663)
XLA Ops:
  0.6 96.5 %shard_map.102 = (bf16[2,4,64,128]{3,2,1,0:T(8,128)(2,1)S(1)}, bf16[2048,512]{1,0:T(8,128)(2,1)S(1)}, bf16[2048,512]{1,0:T(8,128)(2,1)S(1)}, bf16[2048,512]{1,0:T(8,128)(2,1)S(1)}) custom-call(bf16[4,64,256]{2,1,0:T(8,128)(2,1)} %bitcast.5, f32[1,512]{1,0:T(1,128)} %bitcast.6, f32[4,512,512]{2,1,0:T(8,128)} %gate.1, f32[4,512,512]{2,1,0:T(8,128)} %up.1, ...), custom_call_target="tpu_custom_call" | custom-call | tf_op jit(solution)/shard_map/pallas_call | solution.py:725
  97.2 2.8 %shard_map.103 = (bf16[4,64,256]{2,1,0:T(8,128)(2,1)}, bf16[1,2048,512]{2,1,0:T(8,128)(2,1)}, bf16[1,2048,512]{2,1,0:T(8,128)(2,1)}, bf16[1,2048,512]{2,1,0:T(8,128)(2,1)}) custom-call(bf16[2,4,64,128]{3,2,1,0:T(8,128)(2,1)S(1)} %get-tuple-element.12.mixed, bf16[2048,512]{1,0:T(8,128)(2,1)S(1)} %get-tuple-element.13.gate, ...), custom_call_target="tpu_custom_call" | custom-call | tf_op jit(solution)/shard_map/pallas_call | solution.py:703
